TPU v7x, 256 devices: a 4x2x16 block of a 4x16x16 slice. The times are simulated.
256 devices in a mesh: grp: 2 (over y), sp: 32 (over z, core), tp: 4 (over x).
Axes of the slice: x: 4, y: 2, z: 16, core: 2. Of those that a mesh axis runs over, the one named last changes fastest.
The devices are a block of a 4x16x16 slice.
Arguments:
- resid: bfloat16 [12288, 2048], P(('grp', 'sp', 'tp')), parts along dimension 0, may hold values from -6 to 6
- queries: bfloat16 [12288, 1024], P(('grp', 'sp'), 'tp'), parts along dimension 0, may hold values from -64 to 64
- keys: bfloat16 [12288, 256], P(('grp', 'sp'), 'tp'), parts along dimension 0, may hold values from -64 to 64
- values: bfloat16 [12288, 256], P(('grp', 'sp'), 'tp'), parts along dimension 0, may hold values from -6 to 6
- doc_ids: int32 [12288], P(('grp', 'sp')), parts along dimension 0, may hold values from 0 to 15, never falling along the last dimension, each value on 1 to 768 neighbouring positions
- sink_logits: float32 [16], P('tp'), may hold values from 2 to 6
- out_proj: bfloat16 [1024, 2048], P('tp'), may hold values from -1.5 to 1.5
- norm1_gain: float32 [2048], replicated, may hold values from 0.1 to 1.9
- norm1_bias: float32 [2048], replicated, may hold values from -1.8 to 1.8
- route_ids: int32 [12288, 2], P(('grp', 'sp', 'tp')), parts along dimension 0, may hold values from 0 to 31, all different within a row; in each aligned block of 48 rows (0 to 47, 48 to 95, ...) at most 3 rows name the same one
- route_weights: float32 [12288, 2], P(('grp', 'sp', 'tp')), parts along dimension 0, may hold values from 0.25 to 1
- expert_gate: bfloat16 [32, 2048, 3072], P('sp', None, 'tp'), may hold values from -0.125 to 0.125
- expert_up: bfloat16 [32, 2048, 3072], P('sp', None, 'tp'), may hold values from -0.125 to 0.125
- expert_down: bfloat16 [32, 3072, 2048], P('sp', 'tp'), may hold values from -0.109375 to 0.109375
- norm2_gain: float32 [2048], replicated, may hold values from 0.1 to 1.9
- norm2_bias: float32 [2048], replicated, may hold values from -1.8 to 1.8
Outputs:
- mixed: bfloat16 [12288, 2048], P(('grp', 'sp', 'tp')), parts along dimension 0
There are 2 independent parts, one for each index of `grp`. A program takes and returns all parts, laid end to end along the dimension named above; an argument that names none is the same for every part. Nothing has to cross between parts.
Inputs may be any that keep to these rules, and one draw needn't show every extreme that they name: `route_ids`: among the rows of one device (aligned blocks of 48 tokens) no expert is named more than 3 times, a bound that some block reaches; a token's 2 experts differ.
All inputs are finite; a program needn't handle non-finite values.
Results may differ from a plain program's by a relative error of at most 0.012.
Values may be sent and summed in bfloat16 or wider, within the bound.
A program may use at most 64 MiB of HBM per device.

v0:
```python
import jax
import jax.numpy as jnp
from jax import lax
from jax.sharding import Mesh
from jax.sharding import PartitionSpec as P

HEAD_DIM = 64
WINDOW = 128
SP = ("sp_0", "sp_1")
GRP_SP_TP = ("grp", "sp_0", "sp_1", "tp")
GRP_SP = ("grp", "sp_0", "sp_1")


norm_epsilon = 1e-05
residual_scale = 1.4142135623730951
masked_score = -1e30


def with_halo(cells, sides, width):
    for axis, dim in sides:
        count = lax.axis_size(axis)
        ends = count - 1
        head = lax.slice_in_dim(cells, 0, width, axis=dim)
        tail = lax.slice_in_dim(cells, cells.shape[dim] - width, cells.shape[dim], axis=dim)
        cells = jnp.concatenate(
            [
                lax.ppermute(tail, axis, [(i, (i + 1) % count) for i in range(ends)]),
                cells,
                lax.ppermute(head, axis, [((i + 1) % count, i) for i in range(ends)]),
            ],
            axis=dim,
        )
    return cells


def cut_along(shard, dim, size):
    before, after = (shard.shape[:dim], shard.shape[dim + 1 :])
    return jnp.moveaxis(shard.reshape(*before, size, -1, *after), dim, 0)


def sum_at_owner(shard, axis, dim):
    size = lax.axis_size(axis)
    blocks = lax.all_to_all(cut_along(shard, dim, size), axis, 0, 0, tiled=True)
    return jnp.sum(blocks.astype(jnp.float32), axis=0)


def in_order(blocks, dim):
    blocks = jnp.moveaxis(blocks, 0, dim)
    dims = blocks.shape
    return blocks.reshape(*dims[:dim], dims[dim] * dims[dim + 1], *dims[dim + 2 :])


def moved_by_axis(blocks, axes, turns):
    dims = [lax.axis_size(a) for a in axes]
    blocks = blocks.reshape(*dims, *blocks.shape[1:])
    for k in turns:
        blocks = lax.all_to_all(blocks, axes[k], split_axis=k, concat_axis=k, tiled=True)
    return blocks.reshape(-1, *blocks.shape[len(axes) :])


def exchange_by_chip(shard, groups, turns, split_dim, concat_dim):
    size = lax.axis_size(groups[0]) * lax.axis_size(groups[1])
    blocks = cut_along(shard, split_dim, size)
    return in_order(moved_by_axis(blocks, groups, turns), concat_dim)


def sent_to_all(shard, axis):
    copies = jnp.broadcast_to(shard, (lax.axis_size(axis), *shard.shape))
    return lax.all_to_all(copies, axis, split_axis=0, concat_axis=0, tiled=True)


def gathered_copies(shard, axis, dim):
    return in_order(sent_to_all(shard, axis), dim)


def layer_norm(values, gain_vec, bias_vec):
    mean_val = jnp.mean(values, -1, keepdims=True)
    centred = values - mean_val
    variance = jnp.mean(centred * centred, -1, keepdims=True)
    return centred * lax.rsqrt(variance + norm_epsilon) * gain_vec + bias_vec


def per_device(
    resid,
    queries,
    keys,
    values,
    doc_ids,
    sink_logits,
    out_proj,
    norm1_gain,
    norm1_bias,
    route_ids,
    route_weights,
    expert_gate,
    expert_up,
    expert_down,
    norm2_gain,
    norm2_bias,
):
    tok_dev = queries.shape[0]
    local_kv = keys.shape[1] // HEAD_DIM
    local_heads = queries.shape[1] // HEAD_DIM
    groups = local_heads // local_kv
    reach = tok_dev + 2 * WINDOW
    padded_keys, padded_values, padded_docs = (
        with_halo(keys, ((SP, 0),), WINDOW),
        with_halo(values, ((SP, 0),), WINDOW),
        with_halo(doc_ids, ((SP, 0),), WINDOW),
    )
    offset = lax.axis_index(SP) * tok_dev
    seq_total = lax.axis_size(SP) * tok_dev
    query_pos = offset + jnp.arange(tok_dev, dtype=jnp.int32)
    key_pos = offset - WINDOW + jnp.arange(reach, dtype=jnp.int32)
    allowed = (key_pos[None, :] >= 0) & (key_pos[None, :] < seq_total)
    allowed = allowed & (jnp.abs(query_pos[:, None] - key_pos[None, :]) <= WINDOW)
    allowed = allowed & (doc_ids[:, None] == padded_docs[None, :])
    query_heads = queries.reshape(tok_dev, local_kv, groups, HEAD_DIM)
    key_heads = padded_keys.reshape(reach, local_kv, HEAD_DIM)
    value_heads = padded_values.reshape(reach, local_kv, HEAD_DIM)
    sink_local = sink_logits.reshape(local_kv, groups, 1, 1)
    scores = jnp.einsum(
        "qkgd,jkd->kgqj", query_heads, key_heads, preferred_element_type=jnp.float32
    )
    scores = jnp.where(allowed, scores * HEAD_DIM ** (-0.5), masked_score)
    top_score = jnp.maximum(jnp.max(scores, -1, keepdims=True), sink_local)
    raised = jnp.where(allowed, jnp.exp(scores - top_score), 0.0)
    denominator = jnp.exp(sink_local - top_score) + jnp.sum(raised, -1, keepdims=True)
    weights = (raised / denominator).astype(jnp.bfloat16)
    attended = jnp.einsum(
        "kgqj,jkd->qkgd", weights, value_heads, preferred_element_type=jnp.float32
    )
    attended = attended.astype(jnp.bfloat16).reshape(tok_dev, local_heads * HEAD_DIM)
    tok_sub = resid.shape[0]
    row_block = attended
    projected = sum_at_owner(
        jnp.dot(row_block, out_proj, preferred_element_type=jnp.float32).astype(jnp.bfloat16),
        "tp",
        0,
    ).astype(jnp.bfloat16)
    pre_norm = residual_scale * resid.astype(jnp.float32) + projected.astype(jnp.float32)
    normed = layer_norm(pre_norm, norm1_gain, norm1_bias).astype(jnp.bfloat16)
    experts = lax.axis_size(SP)
    capacity = 5 * tok_sub // (2 * experts)
    width = normed.shape[1]
    flat_ids = route_ids.reshape(-1)
    one_hot = (flat_ids[:, None] == jnp.arange(experts, dtype=jnp.int32)[None, :]).astype(jnp.int32)
    ranks = jnp.cumsum(one_hot, axis=0) - 1
    slot_rank = jnp.sum(ranks * one_hot, axis=1)
    slots = flat_ids * capacity + slot_rank
    assignment = slots[None, :] == jnp.arange(experts * capacity, dtype=jnp.int32)[:, None]
    assignment = assignment.reshape(experts * capacity, tok_sub, -1).any(-1).astype(jnp.bfloat16)
    dispatch = jnp.dot(assignment, normed, preferred_element_type=jnp.float32).astype(jnp.bfloat16)
    dispatch = dispatch.reshape(experts, capacity, width)
    arrived = exchange_by_chip(dispatch, ("sp_0", "sp_1"), (1, 0), 0, 0)
    arrived = gathered_copies(arrived[None], "tp", 0)
    flat_rows = arrived.reshape(-1, width)
    gate_weight = expert_gate[0]
    up_weight = expert_up[0]
    down_weight = expert_down[0]
    row_block = flat_rows
    gate_act = jnp.dot(row_block, gate_weight, preferred_element_type=jnp.float32)
    up_act = jnp.dot(row_block, up_weight, preferred_element_type=jnp.float32)
    hidden = (jax.nn.silu(gate_act) * up_act).astype(jnp.bfloat16)
    expert_out = sum_at_owner(
        jnp.dot(hidden, down_weight, preferred_element_type=jnp.float32).astype(jnp.bfloat16),
        "tp",
        0,
    ).astype(jnp.bfloat16)
    returned = exchange_by_chip(
        expert_out.reshape(experts, capacity, width), ("sp_0", "sp_1"), (1, 0), 0, 0
    )
    gathered = jnp.take(returned.reshape(experts * capacity, width), slots, axis=0)
    gathered = gathered.reshape(tok_sub, -1, width).astype(jnp.float32)
    moe_sum = jnp.sum(route_weights[:, :, None] * gathered, axis=1)
    pre_final = residual_scale * normed.astype(jnp.float32) + moe_sum
    return layer_norm(pre_final, norm2_gain, norm2_bias).astype(jnp.bfloat16)


def solution(mesh):
    finer = Mesh(
        mesh.devices.reshape(mesh.shape["grp"], 16, 2, mesh.shape["tp"]),
        ("grp", "sp_0", "sp_1", "tp"),
    )
    placed = (
        P(GRP_SP_TP, None),
        P(GRP_SP, "tp"),
        P(GRP_SP, "tp"),
        P(GRP_SP, "tp"),
        P(GRP_SP),
        P("tp"),
        P("tp", None),
        P(),
        P(),
        P(GRP_SP_TP, None),
        P(GRP_SP_TP, None),
        P(SP, None, "tp"),
        P(SP, None, "tp"),
        P(SP, "tp", None),
        P(),
        P(),
    )
    return jax.shard_map(
        per_device, mesh=finer, in_specs=placed, out_specs=P(GRP_SP_TP, None), check_vma=False
    )
```

profile of v0, /device:TPU:40, one launch (start us, length us, event | category | flops | bytes accessed | tf_op | source)
XLA Modules:
  0.0 223.8 jit_solution(8541807775147488578)
XLA Ops:
  0.9 2.0 collective-permute-start.2
  5.1 5.6 %collective-permute-start.4 = (bf16[128,64]{0,1:T(8,128)(2,1)S(1)}, bf16[128,64]{0,1:T(8,128)(2,1)S(1)}, u32[]{:S(2)}, u32[]{:S(2)}) collective-permute-start(bf16[128,64]{0,1:T(8,128)(2,1)S(1)} %get-tuple-element.9), channel_id=1, source_target_pairs={{0,4},{4,8},{8,12},{12,16},{16,20},{20,24},{24,28},{28,32},{32,36}... | collective-permute-start | bytes 49160 | tf_op jit(solution)/shard_map/ppermute | solution.py:27
  12.8 4.3 %collective-permute-start = (bf16[128,64]{0,1:T(8,128)(2,1)S(1)}, bf16[128,64]{0,1:T(8,128)(2,1)S(1)}, u32[]{:S(2)}, u32[]{:S(2)}) collective-permute-start(bf16[128,64]{0,1:T(8,128)(2,1)S(1)} %get-tuple-element.7), channel_id=1, source_target_pairs={{0,4},{4,8},{8,12},{12,16},{16,20},{20,24},{24,28},{28,32},{32,36}... | collective-permute-start | bytes 49160 | tf_op jit(solution)/shard_map/ppermute | solution.py:27
  22.1 1.4 fusion.44
  26.8 4.7 %all-to-all-start = ((bf16[4,48,2048]{2,1,0:T(8,128)(2,1)}), bf16[4,48,2048]{2,1,0:T(8,128)(2,1)}, u32[]{:S(2)}, u32[]{:S(2)}) async-start(bf16[4,48,2048]{2,1,0:T(8,128)(2,1)} %bitcast.59), calls=%async_computation | async-start | bytes 1572864 | tf_op jit(solution)/shard_map/all_to_all | solution.py:43
  32.8 11.4 %all-to-all-done = bf16[4,48,2048]{2,1,0:T(8,128)(2,1)} async-done(((bf16[4,48,2048]{2,1,0:T(8,128)(2,1)}), bf16[4,48,2048]{2,1,0:T(8,128)(2,1)}, u32[]{:S(2)}, u32[]{:S(2)}) %all-to-all-start) | async-done | bytes 786464 | tf_op jit(solution)/shard_map/all_to_all | solution.py:43
  50.1 4.5 %all_to_all.35 = bf16[16,2,1,3,2048]{4,0,3,2,1:T(8,128)(2,1)S(1)} all-to-all(bf16[16,2,1,3,2048]{4,0,3,2,1:T(8,128)(2,1)S(1)} %copy.63), channel_id=1, replica_groups=mesh['grp'=2,'sp_0'=16,'sp_1'=2,'tp'=4] {'sp_1'}, dimensions={1} | all-to-all | bytes 786432 | tf_op jit(solution)/shard_map/all_to_all | solution.py:57
  55.0 48.6 %all_to_all.36 = bf16[16,2,1,3,2048]{4,1,3,2,0:T(2,128)(2,1)S(1)} all-to-all(bf16[16,2,1,3,2048]{4,1,3,2,0:T(2,128)(2,1)S(1)} %copy.64), channel_id=1, replica_groups=mesh['grp'=2,'sp_0'=16,'sp_1'=2,'tp'=4] {'sp_0'}, dimensions={0} | all-to-all | bytes 786432 | tf_op jit(solution)/shard_map/all_to_all | solution.py:57
  106.0 16.7 %all_to_all.37 = bf16[4,1,32,3,2048]{4,2,3,1,0:T(8,128)(2,1)S(1)} all-to-all(bf16[4,1,32,3,2048]{4,2,3,1,0:T(8,128)(2,1)S(1)} %broadcast_in_dim.28), channel_id=1, replica_groups=mesh['grp'=2,'sp_0'=16,'sp_1'=2,'tp'=4] {'tp'}, dimensions={0} | all-to-all | bytes 3145728 | tf_op jit(solution)/shard_map/all_to_all | solution.py:69
  122.7 2.7 %copy.66 = bf16[4,1,32,3,2048]{4,3,2,0,1:T(4,128)(2,1)} copy(bf16[4,1,32,3,2048]{4,2,3,1,0:T(8,128)(2,1)S(1)} %all_to_all.37) | data formatting | bytes 3145728 | tf_op jit(solution)/shard_map/all_to_all | solution.py:69
  125.3 5.0 %reshape_reshape.3 = bf16[384,2048]{1,0:T(8,128)(2,1)} reshape(bf16[4,1,32,3,2048]{4,3,2,0,1:T(4,128)(2,1)} %copy.66) | data formatting | bytes 3145728 | tf_op jit(solution)/shard_map/reshape;reshape | solution.py:157
  130.4 4.8 %fusion.4 = f32[384,768]{1,0:T(8,128)} fusion(bf16[384,2048]{1,0:T(8,128)(2,1)} %reshape_reshape.3, bf16[1,2048,768]{2,1,0:T(8,128)(2,1)} %param.27), kind=kOutput, calls=%fused_computation.5 | convolution fusion | flops 1207959552 | bytes 5898240 | tf_op jit(solution)/shard_map/dot_general | solution.py:162
  135.1 6.9 %fusion.6 = bf16[384,2048]{1,0:T(8,128)(2,1)} fusion(bf16[1,768,2048]{2,1,0:T(8,128)(2,1)S(1)} %copy-done, bf16[384,2048]{1,0:T(8,128)(2,1)} %reshape_reshape.3, bf16[1,2048,768]{2,1,0:T(8,128)(2,1)} %param.28, f32[384,768]{1,0:T(8,128)} %fusion.4), kind=kOutput, calls=%fused_computation.7 | convolution fusion | flops 2418475008 | bytes 10616832 | tf_op jit(solution)/shard_map/dot_general | solution.py:166
  142.0 18.3 %all_to_all.38 = bf16[4,96,2048]{2,1,0:T(8,128)(2,1)} all-to-all(bf16[4,96,2048]{2,1,0:T(8,128)(2,1)} %bitcast.60), channel_id=1, replica_groups=mesh['grp'=2,'sp_0'=16,'sp_1'=2,'tp'=4] {'tp'}, dimensions={0} | all-to-all | bytes 3145728 | tf_op jit(solution)/shard_map/all_to_all | solution.py:43
  160.3 1.7 reduce_sum.97
  163.0 1.3 copy.67
  164.4 4.1 %all_to_all.39 = bf16[16,2,1,3,2048]{4,0,3,2,1:T(8,128)(2,1)S(1)} all-to-all(bf16[16,2,1,3,2048]{4,0,3,2,1:T(8,128)(2,1)S(1)} %copy.67), channel_id=1, replica_groups=mesh['grp'=2,'sp_0'=16,'sp_1'=2,'tp'=4] {'sp_1'}, dimensions={1} | all-to-all | bytes 786432 | tf_op jit(solution)/shard_map/all_to_all | solution.py:57
  169.6 19.6 %all-to-all-start.6 = ((bf16[16,2,1,3,2048]{4,1,3,2,0:T(2,128)(2,1)}), bf16[16,2,1,3,2048]{4,1,3,2,0:T(2,128)(2,1)S(1)}, u32[]{:S(2)}, u32[]{:S(2)}) async-start(bf16[16,2,1,3,2048]{4,1,3,2,0:T(2,128)(2,1)} %copy.68), calls=%async_computation.6 | async-start | bytes 786432 | tf_op jit(solution)/shard_map/all_to_all | solution.py:57
  191.5 1.4 copy.59
  192.9 20.3 %all-to-all-done.6 = bf16[16,2,1,3,2048]{4,1,3,2,0:T(2,128)(2,1)S(1)} async-done(((bf16[16,2,1,3,2048]{4,1,3,2,0:T(2,128)(2,1)}), bf16[16,2,1,3,2048]{4,1,3,2,0:T(2,128)(2,1)S(1)}, u32[]{:S(2)}, u32[]{:S(2)}) %all-to-all-start.6) | async-done | bytes 393248 | tf_op jit(solution)/shard_map/all_to_all | solution.py:57
  214.3 1.4 reshape_reshape_reshape.11
  215.7 1.6 gather_fusion
  217.2 2.0 gather.7
  219.3 3.2 %multiply_reduce_fusion = f32[48,2048]{1,0:T(8,128)S(1)} fusion(bf16[48,2,2048]{2,1,0:T(2,128)(2,1)} %gather.7, pred[48,2]{1,0:T(8,128)(4,1)S(1)} %copy.62, f32[48,2]{1,0:T(8,128)} %copy.59), kind=kLoop, calls=%fused_computation.18 | loop fusion | flops 688128 | bytes 786912 | tf_op jit(solution)/shard_map/reduce_sum | solution.py:175
  (79 shorter events, 30.1 us)
Async XLA Ops:
  0.0 135.1 %copy-start = (bf16[1,768,2048]{2,1,0:T(8,128)(2,1)S(1)}, bf16[1,768,2048]{2,1,0:T(8,128)(2,1)}, u32[]{:S(2)}) copy-start(bf16[1,768,2048]{2,1,0:T(8,128)(2,1)} %param.29) | copy-start | bytes 9437188
  0.0 23.5 %copy-start.9 = (f32[4]{0:T(128)S(1)}, f32[4]{0:T(128)}, u32[]{:S(2)}) copy-start(f32[4]{0:T(128)} %param.21) | copy-start | bytes 52
  0.9 18.2 %collective-permute-start.2 = (s32[128]{0:T(128)S(1)}, s32[128]{0:T(128)S(1)}, u32[]{:S(2)}, u32[]{:S(2)}) collective-permute-start(s32[128]{0:T(128)S(1)} %get-tuple-element.11), channel_id=1, source_target_pairs={{0,4},{4,8},{8,12},{12,16},{16,20},{20,24},{24,28},{28,32},{32,36}... | collective-permute-start | bytes 1544 | tf_op jit(solution)/shard_map/ppermute | solution.py:27
  2.9 17.5 %collective-permute-start.3 = (s32[128]{0:T(128)S(1)}, s32[128]{0:T(128)S(1)}, u32[]{:S(2)}, u32[]{:S(2)}) collective-permute-start(s32[128]{0:T(128)S(1)} %get-tuple-element.12), channel_id=1, source_target_pairs={{4,0},{8,4},{12,8},{16,12},{20,16},{24,20},{28,24},{32,28},{36,32}... | collective-permute-start | bytes 1544 | tf_op jit(solution)/shard_map/ppermute | solution.py:29
  5.1 17.0 %collective-permute-start.4 = (bf16[128,64]{0,1:T(8,128)(2,1)S(1)}, bf16[128,64]{0,1:T(8,128)(2,1)S(1)}, u32[]{:S(2)}, u32[]{:S(2)}) collective-permute-start(bf16[128,64]{0,1:T(8,128)(2,1)S(1)} %get-tuple-element.9), channel_id=1, source_target_pairs={{0,4},{4,8},{8,12},{12,16},{16,20},{20,24},{24,28},{28,32},{32,36}... | collective-permute-start | bytes 49160 | tf_op jit(solution)/shard_map/ppermute | solution.py:27
  10.7 11.4 %collective-permute-start.5 = (bf16[128,64]{0,1:T(8,128)(2,1)S(1)}, bf16[128,64]{0,1:T(8,128)(2,1)S(1)}, u32[]{:S(2)}, u32[]{:S(2)}) collective-permute-start(bf16[128,64]{0,1:T(8,128)(2,1)S(1)} %get-tuple-element.10), channel_id=1, source_target_pairs={{4,0},{8,4},{12,8},{16,12},{20,16},{24,20},{28,24},{32,28},{36,32}... | collective-permute-start | bytes 49160 | tf_op jit(solution)/shard_map/ppermute | solution.py:29
  12.8 11.4 %collective-permute-start = (bf16[128,64]{0,1:T(8,128)(2,1)S(1)}, bf16[128,64]{0,1:T(8,128)(2,1)S(1)}, u32[]{:S(2)}, u32[]{:S(2)}) collective-permute-start(bf16[128,64]{0,1:T(8,128)(2,1)S(1)} %get-tuple-element.7), channel_id=1, source_target_pairs={{0,4},{4,8},{8,12},{12,16},{16,20},{20,24},{24,28},{28,32},{32,36}... | collective-permute-start | bytes 49160 | tf_op jit(solution)/shard_map/ppermute | solution.py:27
  19.1 5.2 %collective-permute-start.1 = (bf16[128,64]{0,1:T(8,128)(2,1)S(1)}, bf16[128,64]{0,1:T(8,128)(2,1)S(1)}, u32[]{:S(2)}, u32[]{:S(2)}) collective-permute-start(bf16[128,64]{0,1:T(8,128)(2,1)S(1)} %get-tuple-element.8), channel_id=1, source_target_pairs={{4,0},{8,4},{12,8},{16,12},{20,16},{24,20},{28,24},{32,28},{36,32}... | collective-permute-start | bytes 49160 | tf_op jit(solution)/shard_map/ppermute | solution.py:29
  22.1 2.2 copy-start.5
  24.2 1.2 copy-start.4
  25.5 6.6 %copy-start.6 = (s32[48,2]{0,1:T(2,128)S(1)}, s32[48,2]{0,1:T(2,128)}, u32[]{:S(2)}) copy-start(s32[48,2]{0,1:T(2,128)} %param.25) | copy-start | bytes 1156
  26.8 18.7 %copy-start.3 = (bf16[48,2048]{1,0:T(8,128)(2,1)S(1)}, bf16[48,2048]{1,0:T(8,128)(2,1)}, u32[]{:S(2)}) copy-start(bf16[48,2048]{1,0:T(8,128)(2,1)} %param.16) | copy-start | bytes 589828
  26.8 17.4 %all-to-all-start = ((bf16[4,48,2048]{2,1,0:T(8,128)(2,1)}), bf16[4,48,2048]{2,1,0:T(8,128)(2,1)}, u32[]{:S(2)}, u32[]{:S(2)}) async-start(bf16[4,48,2048]{2,1,0:T(8,128)(2,1)} %bitcast.59), calls=%async_computation | async-start | bytes 1572864 | tf_op jit(solution)/shard_map/all_to_all | solution.py:43
  46.7 0.7 copy-start.1
  169.6 43.6 %all-to-all-start.6 = ((bf16[16,2,1,3,2048]{4,1,3,2,0:T(2,128)(2,1)}), bf16[16,2,1,3,2048]{4,1,3,2,0:T(2,128)(2,1)S(1)}, u32[]{:S(2)}, u32[]{:S(2)}) async-start(bf16[16,2,1,3,2048]{4,1,3,2,0:T(2,128)(2,1)} %copy.68), calls=%async_computation.6 | async-start | bytes 786432 | tf_op jit(solution)/shard_map/all_to_all | solution.py:57
  217.2 5.3 %copy-start.2 = (bf16[48,2048]{1,0:T(8,128)(2,1)S(1)}, bf16[48,2048]{1,0:T(8,128)(2,1)}, u32[]{:S(2)}) copy-start(bf16[48,2048]{1,0:T(8,128)(2,1)} %copy-done.1) | copy-start | bytes 589828
  217.2 5.7 %copy-start.7 = (f32[2048]{0:T(1024)S(1)}, f32[2048]{0:T(1024)}, u32[]{:S(2)}) copy-start(f32[2048]{0:T(1024)} %param.31) | copy-start | bytes 24580
  217.2 5.7 %copy-start.8 = (f32[2048]{0:T(1024)S(1)}, f32[2048]{0:T(1024)}, u32[]{:S(2)}) copy-start(f32[2048]{0:T(1024)} %param.30) | copy-start | bytes 24580
where the time goes:
time: 225 us; the launch traced here: 224 us
  blocking collectives  92.2 us (41%)
  starting transfers between devices  40 us (18%)
  local copies, waits for them, and re-layouts  32.1 us (14%)
  waiting for transfers between devices  31.7 us (14%)
  matrix products  15.2 us (7%)
  other arithmetic  12.1 us (5%)
    all_to_all x3, blocking collectives, moved_by_axis(): lax.all_to_all(blocks, axes[k], split_axis=k, concat_axis=k, tiled=True)  57.2 us
    all_to_all x1, waiting for transfers between devices, moved_by_axis(): lax.all_to_all(blocks, axes[k], split_axis=k, concat_axis=k, tiled=True)  20.3 us
    all_to_all x1, starting transfers between devices, moved_by_axis(): lax.all_to_all(blocks, axes[k], split_axis=k, concat_axis=k, tiled=True)  19.6 us
    all_to_all x1, blocking collectives, sum_at_owner(): blocks = lax.all_to_all(cut_along(shard, dim, size), axis, 0, 0, tiled=True)  18.3 us
    all_to_all x1, blocking collectives, sent_to_all(): return lax.all_to_all(copies, axis, split_axis=0, concat_axis=0, tiled=True)  16.7 us
    ppermute x3, starting transfers between devices, with_halo(): lax.ppermute(tail, axis, [(i, (i + 1) % count) for i in range(ends)])  11.8 us
    all_to_all x1, waiting for transfers between devices, sum_at_owner(): blocks = lax.all_to_all(cut_along(shard, dim, size), axis, 0, 0, tiled=True)  11.4 us
    dot_general x1, matrix products, per_device(): jnp.dot(hidden, down_weight, preferred_element_type=jnp.float32)  6.88 us
  transfers between devices with their start and end apart: 8, of which 2 were waited for; matrix products, arithmetic and copies ran while one was open for 6% of the time, Pallas kernels for 0%

commit v1 on v0

v1 whole, which is shorter than its diff:
```python
import functools

import jax
import jax.numpy as jnp
from jax import lax
from jax.experimental import pallas as pl
from jax.experimental.pallas import tpu as pltpu
from jax.sharding import PartitionSpec as P

HEAD_DIM = 64
WINDOW = 128
LANES = 128
GROUPS = 4
EPS = 1e-05
ROOT2 = 1.4142135623730951
MASKED = -1e30
MESH = pl.DeviceIdType.MESH
F32 = jnp.float32
BF16 = jnp.bfloat16


def offsets_far_first(nz):
    order = [nz // 2]
    for d in range(nz // 2 - 1, 0, -1):
        order += [d, -d]
    return order + [0]


def remote(src, dst, send_sem, recv_sem, device):
    return pltpu.make_async_remote_copy(
        src_ref=src, dst_ref=dst, send_sem=send_sem, recv_sem=recv_sem,
        device_id=device, device_id_type=MESH,
    )


def layer_norm(cells, gain, bias):
    mean = jnp.mean(cells, -1, keepdims=True)
    centred = cells - mean
    variance = jnp.mean(centred * centred, -1, keepdims=True)
    return centred * lax.rsqrt(variance + EPS) * gain + bias


def kernel(
    n_sp, cap,
    resid, queries, keys, values, docs, sinks, out_proj_hbm, gain1, bias1,
    route_ids, route_weights, gate_hbm, up_hbm, down_hbm, gain2, bias2,
    out,
    gate, up, down, out_proj, kk, vv, doc_own, doc_halo, attended,
    proj_part, proj_in, proj_left, proj_right, normed,
    wide, table, arrived, rows, hidden, part, sum_in, from_left, from_right,
    result, returned, acc,
    load_sems, halo_send, halo_recv, proj_send, proj_recv,
    z_send, z_recv, ag_send, ag_recv, rs_send, rs_recv, back_send, back_recv,
):
    sp = lax.axis_index("sp")
    tp = lax.axis_index("tp")
    n_tp = 4
    nz = n_sp // 2
    z, core = sp // 2, sp % 2
    right, left = (tp + 1) % n_tp, (tp + n_tp - 1) % n_tp
    to_right, to_left = {"tp": right}, {"tp": left}
    ahead, behind = (sp + 1) % n_sp, (sp + n_sp - 1) % n_sp
    tok_dev = queries.shape[0]
    tok_sub, width = resid.shape
    cut = width // LANES
    unit = cap * cut
    own_pad = kk.shape[0] - 2 * WINDOW
    order = offsets_far_first(nz)
    per_group = nz // GROUPS
    slots = 2 * per_group
    half = slots // 2 * unit
    whole = slots * unit
    n_rows = n_tp * slots * cap

    loads = [
        pltpu.make_async_copy(out_proj_hbm, out_proj, load_sems.at[0]),
        pltpu.make_async_copy(gate_hbm.at[0], gate, load_sems.at[1]),
        pltpu.make_async_copy(up_hbm.at[0], up, load_sems.at[2]),
        pltpu.make_async_copy(down_hbm.at[0], down, load_sems.at[3]),
    ]

    barrier = pltpu.get_barrier_semaphore()

    def greet(i, carry):
        pl.semaphore_signal(barrier, inc=1, device_id={"sp": (sp + i) % n_sp}, device_id_type=MESH)
        return carry

    lax.fori_loop(1, n_sp, greet, 0)
    pl.semaphore_signal(barrier, inc=1, device_id=to_right, device_id_type=MESH)
    pl.semaphore_signal(barrier, inc=1, device_id=to_left, device_id_type=MESH)
    for load in loads:
        load.start()

    k_own, v_own = keys[...], values[...]
    kk[pl.ds(0, tok_dev), :] = jnp.concatenate([k_own, k_own], axis=1)
    vv[pl.ds(0, tok_dev), :] = jnp.concatenate([v_own, v_own], axis=1)
    if own_pad > tok_dev:
        pad = jnp.zeros((own_pad - tok_dev, LANES), BF16)
        kk[pl.ds(tok_dev, own_pad - tok_dev), :] = pad
        vv[pl.ds(tok_dev, own_pad - tok_dev), :] = pad
    doc_own[...] = jnp.broadcast_to(docs[...], doc_own.shape)

    pl.semaphore_wait(barrier, n_sp + 1)

    tail = pl.ds(tok_dev - WINDOW, WINDOW)
    head = pl.ds(0, WINDOW)
    prev_slot, next_slot = pl.ds(own_pad, WINDOW), pl.ds(own_pad + WINDOW, WINDOW)
    halos = []
    for i, (src, dst, peer) in enumerate([
        (kk.at[tail], kk.at[prev_slot], ahead),
        (kk.at[head], kk.at[next_slot], behind),
        (doc_own, doc_halo.at[0], ahead),
        (doc_own, doc_halo.at[1], behind),
        (vv.at[tail], vv.at[prev_slot], ahead),
        (vv.at[head], vv.at[next_slot], behind),
    ]):
        copy = remote(src, dst, halo_send.at[i], halo_recv.at[i], {"sp": peer})
        copy.start()
        halos.append(copy)

    ids = route_ids[...].astype(F32)
    sub_i = lax.broadcasted_iota(jnp.int32, (tok_sub, tok_sub), 0)
    lane_i = lax.broadcasted_iota(jnp.int32, (tok_sub, tok_sub), 1)
    id_col = [ids[:, k : k + 1] for k in range(2)]
    id_row = [
        jnp.sum(jnp.where(sub_i == lane_i, c, 0.0), axis=0, keepdims=True) for c in id_col
    ]
    slot_row, slot_col = [], []
    for k in range(2):
        row, col = cap * id_row[k], cap * id_col[k]
        for other in range(2):
            same_row = (id_col[other] == id_row[k]) & (sub_i < lane_i)
            row = row + jnp.sum(jnp.where(same_row, 1.0, 0.0), axis=0, keepdims=True)
            same_col = (id_col[k] == id_row[other]) & (lane_i < sub_i)
            col = col + jnp.sum(jnp.where(same_col, 1.0, 0.0), axis=1, keepdims=True)
        slot_row.append(row)
        slot_col.append(col)
    n_slots = n_sp * cap
    slot_sub = lax.broadcasted_iota(jnp.int32, (n_slots, tok_sub), 0).astype(F32)
    slot_lane = lax.broadcasted_iota(jnp.int32, (tok_sub, n_slots), 1).astype(F32)
    assign = jnp.where(
        (slot_sub == slot_row[0]) | (slot_sub == slot_row[1]), 1.0, 0.0
    ).astype(BF16)
    choose = [jnp.where(slot_lane == c, 1.0, 0.0).astype(BF16) for c in slot_col]

    reach = own_pad + 2 * WINDOW
    for copy in halos[:4]:
        copy.wait_recv()
    doc_prev = doc_halo[0][0:1, :][:, tok_dev - WINDOW : tok_dev].astype(F32)
    doc_next = doc_halo[1][0:1, :][:, 0:WINDOW].astype(F32)
    doc_here = doc_own[0:1, :].astype(F32)
    if own_pad > tok_dev:
        doc_here = jnp.concatenate([doc_here, jnp.full((1, own_pad - tok_dev), -1.0, F32)], axis=1)
    doc_keys = jnp.concatenate([doc_here, doc_prev, doc_next], axis=1)
    q_sub = lax.broadcasted_iota(jnp.int32, (tok_dev, tok_dev), 0)
    q_lane = lax.broadcasted_iota(jnp.int32, (tok_dev, tok_dev), 1)
    doc_col = jnp.sum(
        jnp.where(q_sub == q_lane, doc_own[0:1, :].astype(F32), 0.0), axis=1, keepdims=True
    )
    lane = lax.broadcasted_iota(jnp.int32, (tok_dev, reach), 1)
    query = lax.broadcasted_iota(jnp.int32, (tok_dev, reach), 0)
    place = jnp.where(
        lane < own_pad, lane,
        jnp.where(lane < own_pad + WINDOW, lane - (own_pad + WINDOW), lane - (own_pad + WINDOW) + tok_dev),
    )
    at = place + sp * tok_dev
    allowed = (at >= 0) & (at < n_sp * tok_dev) & (jnp.abs(query - place) <= WINDOW)
    allowed = allowed & (doc_col == doc_keys)
    for copy in halos[4:]:
        copy.wait_recv()
    pair_lane = lax.broadcasted_iota(jnp.int32, (tok_dev, LANES), 1)
    for pair in range(queries.shape[1] // LANES):
        q_pair = queries[:, pair * LANES : (pair + 1) * LANES]
        outs = []
        for side in range(2):
            mine = (pair_lane < HEAD_DIM) if side == 0 else (pair_lane >= HEAD_DIM)
            q = jnp.where(mine, q_pair.astype(F32) * HEAD_DIM ** (-0.5), 0.0).astype(BF16)
            scores = lax.dot_general(
                q, kk[...], (((1,), (1,)), ((), ())), preferred_element_type=F32
            )
            scores = jnp.where(allowed, scores, MASKED)
            sink = sinks[2 * pair + side]
            top = jnp.maximum(jnp.max(scores, -1, keepdims=True), sink)
            raised = jnp.exp(scores - top)
            total = jnp.exp(sink - top) + jnp.sum(raised, -1, keepdims=True)
            weights = (raised * (1.0 / total)).astype(BF16)
            outs.append(jnp.dot(weights, vv[...], preferred_element_type=F32))
        attended[:, pair * LANES : (pair + 1) * LANES] = jnp.where(
            pair_lane < HEAD_DIM, outs[0], outs[1]
        ).astype(BF16)

    loads[0].wait()
    wide_half = width // 2
    opposite = (tp + 2) % n_tp

    def project(owner, j, h):
        block = attended[pl.ds(pl.multiple_of(owner * tok_sub, tok_sub), tok_sub), :]
        proj_part[j, h] = jnp.dot(
            block, out_proj[:, h * wide_half : (h + 1) * wide_half], preferred_element_type=F32
        ).astype(BF16)

    project(opposite, 3, 0)
    project(opposite, 3, 1)
    c_opp0 = remote(proj_part.at[3, 0], proj_in.at[0], proj_send.at[0], proj_recv.at[0], to_right)
    c_opp0.start()
    c_opp1 = remote(proj_part.at[3, 1], proj_in.at[1], proj_send.at[1], proj_recv.at[1], to_left)
    c_opp1.start()
    project(right, 2, 1)
    project(left, 1, 0)
    c_right1 = remote(proj_part.at[2, 1], proj_left.at[1], proj_send.at[2], proj_recv.at[2], to_right)
    c_right1.start()
    c_left0 = remote(proj_part.at[1, 0], proj_right.at[0], proj_send.at[3], proj_recv.at[3], to_left)
    c_left0.start()
    project(right, 2, 0)
    project(left, 1, 1)
    c_opp0.wait_recv()
    proj_part[2, 0] = (proj_part[2, 0].astype(F32) + proj_in[0].astype(F32)).astype(BF16)
    c_right0 = remote(proj_part.at[2, 0], proj_left.at[0], proj_send.at[4], proj_recv.at[4], to_right)
    c_right0.start()
    c_opp1.wait_recv()
    proj_part[1, 1] = (proj_part[1, 1].astype(F32) + proj_in[1].astype(F32)).astype(BF16)
    c_left1 = remote(proj_part.at[1, 1], proj_right.at[1], proj_send.at[5], proj_recv.at[5], to_left)
    c_left1.start()
    project(tp, 0, 0)
    project(tp, 0, 1)
    for copy in (c_right1, c_left0, c_right0, c_left1):
        copy.wait_recv()
    for h in range(2):
        cols = slice(h * wide_half, (h + 1) * wide_half)
        projected = (
            proj_part[0, h].astype(F32) + proj_left[h].astype(F32) + proj_right[h].astype(F32)
        ).astype(BF16)
        acc[:, cols] = ROOT2 * resid[:, cols].astype(F32) + projected.astype(F32)
    normed[...] = layer_norm(acc[...], gain1[...], bias1[...]).astype(BF16)

    for c in range(0, cut, 2):
        picked = jnp.dot(
            assign, normed[:, c * LANES : (c + 2) * LANES], preferred_element_type=F32
        )
        wide[pl.ds(c, n_slots, stride=cut), :] = picked[:, :LANES]
        wide[pl.ds(c + 1, n_slots, stride=cut), :] = picked[:, LANES:]
    for e in range(n_sp):
        table[e] = wide[pl.ds(e * unit, unit), :].astype(BF16)

    def place_of(g, i):
        return pl.ds((2 * i) * unit, unit), pl.ds((2 * i + 1) * unit, unit)

    for g in range(GROUPS):
        for i in range(per_group):
            o = order[g * per_group + i]
            if o == 0:
                dst = arrived.at[g, 0, pl.ds(2 * i * unit, unit)]
                partner = 2 * z + 1 - core
                remote(table.at[partner], dst, z_send.at[g], z_recv.at[g], {"sp": partner}).start()
            else:
                zd = (z + o + nz) % nz
                at_slot = pl.multiple_of((2 * i + core) * unit, unit)
                for cd in range(2):
                    e = 2 * zd + cd
                    dst = arrived.at[g, 0, pl.ds(at_slot, unit)]
                    remote(table.at[e], dst, z_send.at[g], z_recv.at[g], {"sp": e}).start()

    first, second = pl.ds(0, half), pl.ds(half, half)
    remote_z = [whole] * (GROUPS - 1) + [whole - unit]

    def z_done(g):
        region = arrived.at[g, 0, pl.ds(0, remote_z[g])]
        return remote(region, region, z_send.at[g], z_recv.at[g], to_right)

    ag_copies, rs_copies = [], []

    def ag(i, g, src, dst, device):
        copy = remote(src, dst, ag_send.at[i, g], ag_recv.at[i, g], device)
        ag_copies.append(copy)
        return copy

    def rs(i, g, src, dst, device):
        copy = remote(src, dst, rs_send.at[i, g], rs_recv.at[i, g], device)
        rs_copies.append(copy)
        return copy

    out_of = {}

    def step1(g):
        z_done(g).wait_recv()
        if g == GROUPS - 1:
            arrived[g, 0, pl.ds(whole - unit, unit), :] = table[sp]
        a = ag(0, g, arrived.at[g, 0], arrived.at[g, 1], to_right)
        a.start()
        b = ag(1, g, arrived.at[g, 0], arrived.at[g, 2], to_left)
        b.start()
        out_of["one", g] = (a, b)

    def step2(g):
        a, b = out_of["one", g]
        a.wait_recv()
        c = ag(2, g, arrived.at[g, 1, first], arrived.at[g, 3, first], to_right)
        c.start()
        b.wait_recv()
        d = ag(3, g, arrived.at[g, 2, second], arrived.at[g, 3, second], to_left)
        d.start()
        out_of["two", g] = (c, d)

    def step3(g):
        for copy in out_of["two", g]:
            copy.wait_recv()
        for j in range(n_tp):
            wide[pl.ds(j * whole, whole), :] = arrived[g, j].astype(F32)
        for c in range(cut):
            rows[:, c * LANES : (c + 1) * LANES] = wide[pl.ds(c, n_rows, stride=cut), :].astype(BF16)
        if g == 0:
            loads[1].wait()
            loads[2].wait()
            loads[3].wait()
        step = min(256, hidden.shape[1])

        def act(n, carry):
            cols = pl.ds(pl.multiple_of(n * step, step), step)
            a = jnp.dot(rows[...], gate[:, cols], preferred_element_type=F32)
            b = jnp.dot(rows[...], up[:, cols], preferred_element_type=F32)
            hidden[:, cols] = (a / (1.0 + jnp.exp(-a)) * b).astype(BF16)
            return carry

        lax.fori_loop(0, hidden.shape[1] // step, act, 0)
        for n in range(cut // 2):
            y = jnp.dot(
                hidden[...], down[:, n * 256 : (n + 1) * 256], preferred_element_type=F32
            )
            wide[pl.ds(2 * n, n_rows, stride=cut), :] = y[:, :LANES]
            wide[pl.ds(2 * n + 1, n_rows, stride=cut), :] = y[:, LANES:]
        for j in (3, 1, 2, 0):
            part[g, j] = wide[pl.ds(j * whole, whole), :].astype(BF16)
        a = rs(0, g, part.at[g, 3, first], sum_in.at[g, 0], to_right)
        b = rs(1, g, part.at[g, 3, second], sum_in.at[g, 1], to_left)
        c = rs(2, g, part.at[g, 2, second], from_left.at[g, second], to_right)
        d = rs(3, g, part.at[g, 1, first], from_right.at[g, first], to_left)
        for copy in (a, b, c, d):
            copy.start()
        out_of["three", g] = (a, b, c, d)

    def step4(g):
        a, b, c, d = out_of["three", g]
        a.wait_recv()
        part[g, 2, first, :] = (part[g, 2, first, :].astype(F32) + sum_in[g, 0].astype(F32)).astype(BF16)
        e = rs(4, g, part.at[g, 2, first], from_left.at[g, first], to_right)
        e.start()
        b.wait_recv()
        part[g, 1, second, :] = (part[g, 1, second, :].astype(F32) + sum_in[g, 1].astype(F32)).astype(BF16)
        f = rs(5, g, part.at[g, 1, second], from_right.at[g, second], to_left)
        f.start()
        out_of["four", g] = (c, d, e, f)

    def step5(g):
        for copy in out_of["four", g]:
            copy.wait_recv()
        result[g] = (
            part[g, 0].astype(F32) + from_left[g].astype(F32) + from_right[g].astype(F32)
        ).astype(BF16)
        for i in range(per_group):
            o = order[g * per_group + i]
            for cs in range(2):
                src = pl.ds((2 * i + cs) * unit, unit)
                if o == 0 and cs == 1:
                    returned[sp] = result[g, src, :]
                else:
                    peer = 2 * z + 1 - core if o == 0 else 2 * ((z - o + nz) % nz) + cs
                    remote(
                        result.at[g, src], returned.at[sp], back_send.at[g], back_recv.at[0], {"sp": peer}
                    ).start()

    step1(0)
    step2(0)
    step1(1)
    step3(0)
    step2(1)
    step4(0)
    step1(2)
    step3(1)
    step5(0)
    step2(2)
    step4(1)
    step1(3)
    step3(2)
    step5(1)
    step2(3)
    step4(2)
    step3(3)
    step5(2)
    step4(3)
    step5(3)

    region = returned.at[pl.ds(0, n_sp - 1)]
    remote(region, region, back_send.at[0], back_recv.at[0], to_right).wait_recv()
    for e in range(n_sp):
        wide[pl.ds(e * unit, unit), :] = returned[e].astype(F32)
    share = [route_weights[:, k : k + 1] for k in range(2)]
    for c in range(0, cut, 2):
        cols = slice(c * LANES, (c + 2) * LANES)
        cells = jnp.concatenate(
            [wide[pl.ds(c + i, n_slots, stride=cut), :].astype(BF16) for i in range(2)], axis=1
        )
        total = ROOT2 * normed[:, cols].astype(F32)
        moe = share[0] * jnp.dot(choose[0], cells, preferred_element_type=F32)
        moe = moe + share[1] * jnp.dot(choose[1], cells, preferred_element_type=F32)
        acc[:, cols] = total + moe
    out[...] = layer_norm(acc[...], gain2[...], bias2[...]).astype(BF16)

    for copy in halos:
        copy.wait_send()
    for copy in (c_opp0, c_opp1, c_right1, c_left0, c_right0, c_left1):
        copy.wait_send()
    for copy in ag_copies + rs_copies:
        copy.wait_send()
    for g in range(GROUPS):
        z_done(g).wait_send()
        region = result.at[g, pl.ds(0, remote_z[g])]
        remote(region, region, back_send.at[g], back_recv.at[0], to_right).wait_send()


def per_device(
    resid, queries, keys, values, doc_ids, sink_logits, out_proj, norm1_gain, norm1_bias,
    route_ids, route_weights, expert_gate, expert_up, expert_down, norm2_gain, norm2_bias,
):
    n_sp = lax.axis_size("sp")
    tok_dev, att = queries.shape
    tok_sub, width = resid.shape
    ff = expert_gate.shape[2]
    cap = 2 * tok_sub // n_sp
    cut = width // LANES
    unit = cap * cut
    own_pad = -(-tok_dev // LANES) * LANES
    slots = n_sp // GROUPS
    whole = slots * unit
    half = whole // 2
    n_rows = 4 * slots * cap
    vmem = pl.BlockSpec(memory_space=pltpu.VMEM)
    hbm = pl.BlockSpec(memory_space=pl.ANY)
    dma = pltpu.SemaphoreType.DMA
    scratch = [
        pltpu.VMEM((width, ff), BF16),
        pltpu.VMEM((width, ff), BF16),
        pltpu.VMEM((ff, width), BF16),
        pltpu.VMEM((att, width), BF16),
        pltpu.VMEM((own_pad + 2 * WINDOW, LANES), BF16),
        pltpu.VMEM((own_pad + 2 * WINDOW, LANES), BF16),
        pltpu.VMEM((8, tok_dev), jnp.int32),
        pltpu.VMEM((2, 8, tok_dev), jnp.int32),
        pltpu.VMEM((tok_dev, att), BF16),
        pltpu.VMEM((4, 2, tok_sub, width // 2), BF16),
        pltpu.VMEM((2, tok_sub, width // 2), BF16),
        pltpu.VMEM((2, tok_sub, width // 2), BF16),
        pltpu.VMEM((2, tok_sub, width // 2), BF16),
        pltpu.VMEM((tok_sub, width), BF16),
        pltpu.VMEM((max(n_sp * unit, 4 * whole), LANES), F32),
        pltpu.VMEM((n_sp, unit, LANES), BF16),
        pltpu.VMEM((GROUPS, 4, whole, LANES), BF16),
        pltpu.VMEM((n_rows, width), BF16),
        pltpu.VMEM((n_rows, ff), BF16),
        pltpu.VMEM((GROUPS, 4, whole, LANES), BF16),
        pltpu.VMEM((GROUPS, 2, half, LANES), BF16),
        pltpu.VMEM((GROUPS, whole, LANES), BF16),
        pltpu.VMEM((GROUPS, whole, LANES), BF16),
        pltpu.VMEM((GROUPS, whole, LANES), BF16),
        pltpu.VMEM((n_sp, unit, LANES), BF16),
        pltpu.VMEM((tok_sub, width), F32),
        dma((4,)), dma((6,)), dma((6,)), dma((6,)), dma((6,)),
        dma((GROUPS,)), dma((GROUPS,)), dma((4, GROUPS)), dma((4, GROUPS)),
        dma((6, GROUPS)), dma((6, GROUPS)), dma((GROUPS,)), dma((1,)),
    ]
    flops = 2 * tok_dev * att * width + 2 * 4 * tok_sub * 2 * width * ff * 3
    return pl.pallas_call(
        functools.partial(kernel, n_sp, cap),
        out_shape=jax.ShapeDtypeStruct((tok_sub, width), BF16),
        in_specs=[
            vmem, vmem, vmem, vmem, vmem, pl.BlockSpec(memory_space=pltpu.SMEM), hbm,
            vmem, vmem, vmem, vmem, hbm, hbm, hbm, vmem, vmem,
        ],
        out_specs=vmem,
        scratch_shapes=scratch,
        compiler_params=pltpu.CompilerParams(
            collective_id=0, has_side_effects=True, vmem_limit_bytes=56 * 1024 * 1024
        ),
        cost_estimate=pl.CostEstimate(flops=flops, bytes_accessed=12_000_000, transcendentals=0),
        name="layer",
    )(
        resid, queries, keys, values, doc_ids[None, :], sink_logits, out_proj,
        norm1_gain[None, :], norm1_bias[None, :], route_ids, route_weights,
        expert_gate, expert_up, expert_down, norm2_gain[None, :], norm2_bias[None, :],
    )


def solution(mesh):
    rows = ("grp", "sp", "tp")
    placed = (
        P(rows, None),
        P(("grp", "sp"), "tp"),
        P(("grp", "sp"), "tp"),
        P(("grp", "sp"), "tp"),
        P(("grp", "sp")),
        P("tp"),
        P("tp", None),
        P(),
        P(),
        P(rows, None),
        P(rows, None),
        P("sp", None, "tp"),
        P("sp", None, "tp"),
        P("sp", "tp", None),
        P(),
        P(),
    )
    return jax.shard_map(
        per_device, mesh=mesh, in_specs=placed, out_specs=P(rows, None), check_vma=False
    )
```

time: 225 us -> 113 us (0.50)
  Pallas kernels: 0 us -> 105 us
  blocking collectives: 92.2 us -> 0 us
  starting transfers between devices: 40 us -> 0 us
  waiting for transfers between devices: 31.7 us -> 0 us
  local copies, waits for them, and re-layouts: 32.1 us -> 7.31 us
  matrix products: 15.2 us -> 0 us
  other arithmetic: 12.1 us -> 0 us
    pallas_call x0 -> x1, Pallas kernels: none -> 105 us  [per_device(): pl.pallas_call(functools.partial(kernel, n_sp, cap), out_shape=jax.ShapeD...]
    all_to_all x5 -> x0, blocking collectives: 92.2 us -> none  [the longest x3 57.2 us: moved_by_axis(): lax.all_to_all(blocks, axes[k], split_axis=k, concat_axis=k, tiled=True)]
    all_to_all x2 -> x0, waiting for transfers between devices: 31.7 us -> none  [the longest x1 20.3 us: moved_by_axis(): lax.all_to_all(blocks, axes[k], split_axis=k, concat_axis=k, tiled=True)]
    all_to_all x2 -> x0, starting transfers between devices: 24.3 us -> none  [the longest x1 19.6 us: moved_by_axis(): lax.all_to_all(blocks, axes[k], split_axis=k, concat_axis=k, tiled=True)]
    ppermute x6 -> x0, starting transfers between devices: 15.7 us -> none  [the longest x3 11.8 us: with_halo(): lax.ppermute(tail, axis, [(i, (i + 1) % count) for i in range(ends)])]
    dot_general x6 -> x0, matrix products: 15.2 us -> none  [the longest x1 6.88 us: per_device(): jnp.dot(hidden, down_weight, preferred_element_type=jnp.float32)]
    another operation x7 -> x0, local copies, waits for them, and re-layouts: 12 us -> none  [the longest x1 5.03 us: per_device(): flat_rows = arrived.reshape(-1, width)]
    reduce_sum x9 -> x0, other arithmetic: 7.71 us -> none  [the longest x1 3.23 us: per_device(): moe_sum = jnp.sum(route_weights[:, :, None] * gathered, axis=1)]
  transfers between devices with their start and end apart: 8 -> 0, of which waited for: 2 -> 0; matrix products, arithmetic and copies ran while one was open for 6% -> 0% of each run, Pallas kernels for 0% -> 0%
where the time goes in v1:
time: 113 us; the launch traced here: 112 us
  Pallas kernels  105 us (93%)
  local copies, waits for them, and re-layouts  7.31 us (6%)
    pallas_call x1, Pallas kernels, per_device(): pl.pallas_call(functools.partial(kernel, n_sp, cap), out_shape=jax.ShapeD...  105 us
    unnamed x5, local copies, waits for them, and re-layouts  7.31 us

profile of v1, /device:TPU:40, one launch (start us, length us, event | category | flops | bytes accessed | tf_op | source)
XLA Modules:
  0.0 112.0 jit_solution(16935079136063365189)
XLA Ops:
  0.0 1.4 %copy.19.route_ids = s32[48,2]{1,0:T(8,128)} copy(s32[48,2]{0,1:T(2,128)} %param.25) | data formatting | bytes 768 | tf_op args[9]
  1.4 1.4 %copy.20.route_weights = f32[48,2]{1,0:T(8,128)} copy(f32[48,2]{0,1:T(2,128)} %param.26) | data formatting | bytes 768 | tf_op args[10]
  2.7 1.5 %copy.17.keys = bf16[192,64]{1,0:T(8,128)(2,1)} copy(bf16[192,64]{0,1:T(8,128)(2,1)} %param.18) | data formatting | bytes 49152 | tf_op args[2]
  4.2 1.5 %copy.18.values = bf16[192,64]{1,0:T(8,128)(2,1)} copy(bf16[192,64]{0,1:T(8,128)(2,1)} %param.19) | data formatting | bytes 49152 | tf_op args[3]
  5.7 104.7 %layer.1 = bf16[48,2048]{1,0:T(8,128)(2,1)} custom-call(bf16[48,2048]{1,0:T(8,128)(2,1)} %resid.1, bf16[192,256]{1,0:T(8,128)(2,1)} %queries.1, bf16[192,64]{1,0:T(8,128)(2,1)} %copy.17.keys, bf16[192,64]{1,0:T(8,128)(2,1)} %copy.18.values, s32[1,192]{1,0:T(1,128)} %bitcast.9, f32[4]{0:T(128)} %sinks.1, bf16[256,2048]{1,0:T(8,128)(2,1)} %out_proj_hbm.1, ...), custom_call_target="tpu_custom_call" | custom-call | flops 3825205248 | bytes 12000000 | tf_op jit(solution)/shard_map/layer/pallas_call | solution.py:471
  110.4 1.6 %copy.22 = bf16[48,2048]{1,0:T(8,128)(2,1)} copy(bf16[48,2048]{1,0:T(8,128)(2,1)} %layer.1) | data formatting | bytes 393216

commit v2 on v1

--- a/solution.py
+++ b/solution.py
@@ -19,13 +19,6 @@
 BF16 = jnp.bfloat16
 
 
-def offsets_far_first(nz):
-    order = [nz // 2]
-    for d in range(nz // 2 - 1, 0, -1):
-        order += [d, -d]
-    return order + [0]
-
-
 def remote(src, dst, send_sem, recv_sem, device):
     return pltpu.make_async_remote_copy(
         src_ref=src, dst_ref=dst, send_sem=send_sem, recv_sem=recv_sem,
@@ -50,24 +43,25 @@
     wide, table, arrived, rows, hidden, part, sum_in, from_left, from_right,
     result, returned, acc,
     load_sems, halo_send, halo_recv, proj_send, proj_recv,
-    z_send, z_recv, ag_send, ag_recv, rs_send, rs_recv, back_send, back_recv,
+    chain, present, z_send, z_recv, ag_send, ag_recv, rs_send, rs_recv, back_send, back_recv,
 ):
     sp = lax.axis_index("sp")
     tp = lax.axis_index("tp")
     n_tp = 4
-    nz = n_sp // 2
-    z, core = sp // 2, sp % 2
+    core = sp % 2
     right, left = (tp + 1) % n_tp, (tp + n_tp - 1) % n_tp
     to_right, to_left = {"tp": right}, {"tp": left}
-    ahead, behind = (sp + 1) % n_sp, (sp + n_sp - 1) % n_sp
+    last = n_sp - 1
+    partner = sp + 1 - 2 * core
+    across = sp - 1 + 2 * core
+    has_across = (across >= 0) & (across <= last)
     tok_dev = queries.shape[0]
     tok_sub, width = resid.shape
     cut = width // LANES
     unit = cap * cut
+    my_group, my_slot = sp // (n_sp // GROUPS), sp % (n_sp // GROUPS)
     own_pad = kk.shape[0] - 2 * WINDOW
-    order = offsets_far_first(nz)
-    per_group = nz // GROUPS
-    slots = 2 * per_group
+    slots = n_sp // GROUPS
     half = slots // 2 * unit
     whole = slots * unit
     n_rows = n_tp * slots * cap
@@ -81,50 +75,98 @@
 
     barrier = pltpu.get_barrier_semaphore()
 
-    def greet(i, carry):
-        pl.semaphore_signal(barrier, inc=1, device_id={"sp": (sp + i) % n_sp}, device_id_type=MESH)
-        return carry
-
-    lax.fori_loop(1, n_sp, greet, 0)
-    pl.semaphore_signal(barrier, inc=1, device_id=to_right, device_id_type=MESH)
-    pl.semaphore_signal(barrier, inc=1, device_id=to_left, device_id_type=MESH)
+    def tell(sem, device):
+        pl.semaphore_signal(sem, inc=1, device_id=device, device_id_type=MESH)
+
+    tell(barrier, to_right)
+    tell(barrier, to_left)
+    tell(barrier, {"sp": partner})
+
+    @pl.when(has_across)
+    def _():
+        tell(barrier, {"sp": across})
+
     for load in loads:
         load.start()
 
-    k_own, v_own = keys[...], values[...]
-    kk[pl.ds(0, tok_dev), :] = jnp.concatenate([k_own, k_own], axis=1)
-    vv[pl.ds(0, tok_dev), :] = jnp.concatenate([v_own, v_own], axis=1)
+    def doubled(cells):
+        return jnp.transpose(jnp.concatenate([cells, cells], axis=0).astype(F32)).astype(BF16)
+
+    kk[pl.ds(0, tok_dev), :] = doubled(keys[...])
+    vv[pl.ds(0, tok_dev), :] = doubled(values[...])
     if own_pad > tok_dev:
         pad = jnp.zeros((own_pad - tok_dev, LANES), BF16)
         kk[pl.ds(tok_dev, own_pad - tok_dev), :] = pad
         vv[pl.ds(tok_dev, own_pad - tok_dev), :] = pad
     doc_own[...] = jnp.broadcast_to(docs[...], doc_own.shape)
 
-    pl.semaphore_wait(barrier, n_sp + 1)
+    prev_slot, next_slot = pl.ds(own_pad, WINDOW), pl.ds(own_pad + WINDOW, WINDOW)
+
+    def blank(slot, i):
+        kk[slot, :] = jnp.zeros((WINDOW, LANES), BF16)
+        vv[slot, :] = jnp.zeros((WINDOW, LANES), BF16)
+        doc_halo[i] = jnp.zeros(doc_own.shape, jnp.int32)
+
+    @pl.when(sp == 0)
+    def _():
+        blank(prev_slot, 0)
+
+    @pl.when(sp == last)
+    def _():
+        blank(next_slot, 1)
+
+    pl.semaphore_wait(barrier, jnp.where(has_across, 4, 3))
 
     tail = pl.ds(tok_dev - WINDOW, WINDOW)
     head = pl.ds(0, WINDOW)
-    prev_slot, next_slot = pl.ds(own_pad, WINDOW), pl.ds(own_pad + WINDOW, WINDOW)
-    halos = []
-    for i, (src, dst, peer) in enumerate([
-        (kk.at[tail], kk.at[prev_slot], ahead),
-        (kk.at[head], kk.at[next_slot], behind),
-        (doc_own, doc_halo.at[0], ahead),
-        (doc_own, doc_halo.at[1], behind),
-        (vv.at[tail], vv.at[prev_slot], ahead),
-        (vv.at[head], vv.at[next_slot], behind),
-    ]):
-        copy = remote(src, dst, halo_send.at[i], halo_recv.at[i], {"sp": peer})
-        copy.start()
-        halos.append(copy)
+    to_next, to_prev = {"sp": (sp + 1) % n_sp}, {"sp": (sp + last) % n_sp}
+    halos_up = [
+        remote(src, dst, halo_send.at[i], halo_recv.at[i], to_next)
+        for i, (src, dst) in enumerate([
+            (doc_own, doc_halo.at[0]), (kk.at[tail], kk.at[prev_slot]), (vv.at[tail], vv.at[prev_slot]),
+        ])
+    ]
+    halos_down = [
+        remote(src, dst, halo_send.at[i], halo_recv.at[i], to_prev)
+        for i, (src, dst) in enumerate([
+            (doc_own, doc_halo.at[1]), (kk.at[head], kk.at[next_slot]), (vv.at[head], vv.at[next_slot]),
+        ], 3)
+    ]
+
+    @pl.when(sp < last)
+    def _():
+        for copy in halos_up:
+            copy.start()
+
+    @pl.when(sp > 0)
+    def _():
+        for copy in halos_down:
+            copy.start()
+
+    @pl.when(sp > 0)
+    def _():
+        pl.semaphore_wait(chain, 1)
+
+    @pl.when(sp < last)
+    def _():
+        tell(chain, to_next)
+
+    def tell_below(d, carry):
+        tell(present.at[sp], {"sp": d})
+        return carry
+
+    lax.fori_loop(0, sp, tell_below, 0)
 
     ids = route_ids[...].astype(F32)
     sub_i = lax.broadcasted_iota(jnp.int32, (tok_sub, tok_sub), 0)
     lane_i = lax.broadcasted_iota(jnp.int32, (tok_sub, tok_sub), 1)
-    id_col = [ids[:, k : k + 1] for k in range(2)]
-    id_row = [
-        jnp.sum(jnp.where(sub_i == lane_i, c, 0.0), axis=0, keepdims=True) for c in id_col
-    ]
+
+    def upright(row):
+        return jnp.sum(jnp.where(sub_i == lane_i, row, 0.0), axis=1, keepdims=True)
+
+    id_row = [ids[k : k + 1, :] for k in range(2)]
+    id_col = [upright(row) for row in id_row]
+    share = [upright(route_weights[k : k + 1, :]) for k in range(2)]
     slot_row, slot_col = [], []
     for k in range(2):
         row, col = cap * id_row[k], cap * id_col[k]
@@ -144,8 +186,16 @@
     choose = [jnp.where(slot_lane == c, 1.0, 0.0).astype(BF16) for c in slot_col]
 
     reach = own_pad + 2 * WINDOW
-    for copy in halos[:4]:
-        copy.wait_recv()
+    @pl.when(sp > 0)
+    def _():
+        for copy in halos_up:
+            copy.wait_recv()
+
+    @pl.when(sp < last)
+    def _():
+        for copy in halos_down:
+            copy.wait_recv()
+
     doc_prev = doc_halo[0][0:1, :][:, tok_dev - WINDOW : tok_dev].astype(F32)
     doc_next = doc_halo[1][0:1, :][:, 0:WINDOW].astype(F32)
     doc_here = doc_own[0:1, :].astype(F32)
@@ -166,8 +216,6 @@
     at = place + sp * tok_dev
     allowed = (at >= 0) & (at < n_sp * tok_dev) & (jnp.abs(query - place) <= WINDOW)
     allowed = allowed & (doc_col == doc_keys)
-    for copy in halos[4:]:
-        copy.wait_recv()
     pair_lane = lax.broadcasted_iota(jnp.int32, (tok_dev, LANES), 1)
     for pair in range(queries.shape[1] // LANES):
         q_pair = queries[:, pair * LANES : (pair + 1) * LANES]
@@ -241,32 +289,27 @@
         wide[pl.ds(c + 1, n_slots, stride=cut), :] = picked[:, LANES:]
     for e in range(n_sp):
         table[e] = wide[pl.ds(e * unit, unit), :].astype(BF16)
-
-    def place_of(g, i):
-        return pl.ds((2 * i) * unit, unit), pl.ds((2 * i + 1) * unit, unit)
-
-    for g in range(GROUPS):
-        for i in range(per_group):
-            o = order[g * per_group + i]
-            if o == 0:
-                dst = arrived.at[g, 0, pl.ds(2 * i * unit, unit)]
-                partner = 2 * z + 1 - core
-                remote(table.at[partner], dst, z_send.at[g], z_recv.at[g], {"sp": partner}).start()
-            else:
-                zd = (z + o + nz) % nz
-                at_slot = pl.multiple_of((2 * i + core) * unit, unit)
-                for cd in range(2):
-                    e = 2 * zd + cd
-                    dst = arrived.at[g, 0, pl.ds(at_slot, unit)]
-                    remote(table.at[e], dst, z_send.at[g], z_recv.at[g], {"sp": e}).start()
+    my_place = pl.ds(pl.multiple_of(my_slot * unit, unit), unit)
+    arrived[my_group, 0, my_place, :] = table[sp]
+
+    def dispatch(d):
+        remote(
+            table.at[d], arrived.at[my_group, 0, my_place], z_send.at[0], z_recv.at[sp], {"sp": d}
+        ).start()
+
+    def dispatch_down(i, carry):
+        dispatch(sp - i)
+        return carry
+
+    def dispatch_up(d, carry):
+        pl.semaphore_wait(present.at[d], 1)
+        dispatch(d)
+        return carry
+
+    lax.fori_loop(1, sp + 1, dispatch_down, 0)
+    lax.fori_loop(sp + 1, n_sp, dispatch_up, 0)
 
     first, second = pl.ds(0, half), pl.ds(half, half)
-    remote_z = [whole] * (GROUPS - 1) + [whole - unit]
-
-    def z_done(g):
-        region = arrived.at[g, 0, pl.ds(0, remote_z[g])]
-        return remote(region, region, z_send.at[g], z_recv.at[g], to_right)
-
     ag_copies, rs_copies = [], []
 
     def ag(i, g, src, dst, device):
@@ -282,9 +325,14 @@
     out_of = {}
 
     def step1(g):
-        z_done(g).wait_recv()
-        if g == GROUPS - 1:
-            arrived[g, 0, pl.ds(whole - unit, unit), :] = table[sp]
+        for i in range(slots):
+            s = g * slots + i
+            place = arrived.at[g, 0, pl.ds(i * unit, unit)]
+
+            @pl.when(s != sp)
+            def _():
+                remote(place, place, z_send.at[0], z_recv.at[s], to_right).wait_recv()
+
         a = ag(0, g, arrived.at[g, 0], arrived.at[g, 1], to_right)
         a.start()
         b = ag(1, g, arrived.at[g, 0], arrived.at[g, 2], to_left)
@@ -356,28 +404,30 @@
         result[g] = (
             part[g, 0].astype(F32) + from_left[g].astype(F32) + from_right[g].astype(F32)
         ).astype(BF16)
-        for i in range(per_group):
-            o = order[g * per_group + i]
-            for cs in range(2):
-                src = pl.ds((2 * i + cs) * unit, unit)
-                if o == 0 and cs == 1:
-                    returned[sp] = result[g, src, :]
-                else:
-                    peer = 2 * z + 1 - core if o == 0 else 2 * ((z - o + nz) % nz) + cs
-                    remote(
-                        result.at[g, src], returned.at[sp], back_send.at[g], back_recv.at[0], {"sp": peer}
-                    ).start()
+        for i in range(slots):
+            s = g * slots + i
+            src = pl.ds(i * unit, unit)
+
+            @pl.when(s != sp)
+            def _():
+                remote(
+                    result.at[g, src], returned.at[sp], back_send.at[0], back_recv.at[0], {"sp": s}
+                ).start()
+
+            @pl.when(s == sp)
+            def _():
+                returned[sp] = result[g, src, :]
 
     step1(0)
     step2(0)
     step1(1)
     step3(0)
     step2(1)
+    step1(2)
     step4(0)
-    step1(2)
     step3(1)
+    step2(2)
     step5(0)
-    step2(2)
     step4(1)
     step1(3)
     step3(2)
@@ -389,11 +439,10 @@
     step4(3)
     step5(3)
 
-    region = returned.at[pl.ds(0, n_sp - 1)]
-    remote(region, region, back_send.at[0], back_recv.at[0], to_right).wait_recv()
+    others = returned.at[pl.ds(0, last)]
+    remote(others, others, back_send.at[0], back_recv.at[0], to_right).wait_recv()
     for e in range(n_sp):
         wide[pl.ds(e * unit, unit), :] = returned[e].astype(F32)
-    share = [route_weights[:, k : k + 1] for k in range(2)]
     for c in range(0, cut, 2):
         cols = slice(c * LANES, (c + 2) * LANES)
         cells = jnp.concatenate(
@@ -405,16 +454,22 @@
         acc[:, cols] = total + moe
     out[...] = layer_norm(acc[...], gain2[...], bias2[...]).astype(BF16)
 
-    for copy in halos:
-        copy.wait_send()
+    @pl.when(sp < last)
+    def _():
+        for copy in halos_up:
+            copy.wait_send()
+
+    @pl.when(sp > 0)
+    def _():
+        for copy in halos_down:
+            copy.wait_send()
+
     for copy in (c_opp0, c_opp1, c_right1, c_left0, c_right0, c_left1):
         copy.wait_send()
     for copy in ag_copies + rs_copies:
         copy.wait_send()
-    for g in range(GROUPS):
-        z_done(g).wait_send()
-        region = result.at[g, pl.ds(0, remote_z[g])]
-        remote(region, region, back_send.at[g], back_recv.at[0], to_right).wait_send()
+    remote(others, others, z_send.at[0], z_recv.at[0], to_right).wait_send()
+    remote(others, others, back_send.at[0], back_recv.at[0], to_right).wait_send()
 
 
 def per_device(
@@ -464,8 +519,9 @@
         pltpu.VMEM((n_sp, unit, LANES), BF16),
         pltpu.VMEM((tok_sub, width), F32),
         dma((4,)), dma((6,)), dma((6,)), dma((6,)), dma((6,)),
-        dma((GROUPS,)), dma((GROUPS,)), dma((4, GROUPS)), dma((4, GROUPS)),
-        dma((6, GROUPS)), dma((6, GROUPS)), dma((GROUPS,)), dma((1,)),
+        pltpu.SemaphoreType.REGULAR, pltpu.SemaphoreType.REGULAR((n_sp,)),
+        dma((1,)), dma((n_sp,)), dma((4, GROUPS)), dma((4, GROUPS)),
+        dma((6, GROUPS)), dma((6, GROUPS)), dma((1,)), dma((1,)),
     ]
     flops = 2 * tok_dev * att * width + 2 * 4 * tok_sub * 2 * width * ff * 3
     return pl.pallas_call(
@@ -483,8 +539,8 @@
         cost_estimate=pl.CostEstimate(flops=flops, bytes_accessed=12_000_000, transcendentals=0),
         name="layer",
     )(
-        resid, queries, keys, values, doc_ids[None, :], sink_logits, out_proj,
-        norm1_gain[None, :], norm1_bias[None, :], route_ids, route_weights,
+        resid, queries, keys.T, values.T, doc_ids[None, :], sink_logits, out_proj,
+        norm1_gain[None, :], norm1_bias[None, :], route_ids.T, route_weights.T,
         expert_gate, expert_up, expert_down, norm2_gain[None, :], norm2_bias[None, :],
     )
 

time: 113 us -> 104 us (0.920)
  the two profiles are of different devices: /device:TPU:40 before, /device:TPU:33 now
where the time goes in v2:
time: 104 us
  Pallas kernels  102 us (98%)
  local copies, waits for them, and re-layouts  1.62 us (2%)
    pallas_call x1, Pallas kernels, per_device(): pl.pallas_call(functools.partial(kernel, n_sp, cap), out_shape=jax.ShapeD...  102 us

profile of v2, /device:TPU:33, one launch (start us, length us, event | category | flops | bytes accessed | tf_op | source)
XLA Modules:
  0.0 103.7 jit_solution(5438819800871387103)
XLA Ops:
  0.0 102.1 %layer.1 = bf16[48,2048]{1,0:T(8,128)(2,1)} custom-call(bf16[48,2048]{1,0:T(8,128)(2,1)} %resid.1, bf16[192,256]{1,0:T(8,128)(2,1)} %queries.1, bf16[64,192]{1,0:T(8,128)(2,1)} %bitcast.9, bf16[64,192]{1,0:T(8,128)(2,1)} %bitcast.10, s32[1,192]{1,0:T(1,128)} %bitcast.15, f32[4]{0:T(128)} %sinks.1, bf16[256,2048]{1,0:T(8,128)(2,1)} %out_proj_hbm.1, ...), custom_call_target="tpu_custom_call" | custom-call | flops 3825205248 | bytes 12000000 | tf_op jit(solution)/shard_map/layer/pallas_call | solution.py:527
  102.1 1.6 %copy.18 = bf16[48,2048]{1,0:T(8,128)(2,1)} copy(bf16[48,2048]{1,0:T(8,128)(2,1)} %layer.1) | data formatting | bytes 393216

commit v3 on v2

--- a/solution.py
+++ b/solution.py
@@ -10,13 +10,22 @@
 HEAD_DIM = 64
 WINDOW = 128
 LANES = 128
-GROUPS = 4
 EPS = 1e-05
 ROOT2 = 1.4142135623730951
 MASKED = -1e30
 MESH = pl.DeviceIdType.MESH
 F32 = jnp.float32
 BF16 = jnp.bfloat16
+
+
+def groups_of(nz):
+    base, extra = nz // 4, nz // 16
+    edges = (0, base + extra, 2 * base + extra, 3 * base + extra, nz)
+    return tuple(zip(edges[:-1], edges[1:]))
+
+
+def offset_of(i):
+    return (i + 1) // 2 if i % 2 else -(i // 2)
 
 
 def remote(src, dst, send_sem, recv_sem, device):
@@ -43,28 +52,41 @@
     wide, table, arrived, rows, hidden, part, sum_in, from_left, from_right,
     result, returned, acc,
     load_sems, halo_send, halo_recv, proj_send, proj_recv,
-    chain, present, z_send, z_recv, ag_send, ag_recv, rs_send, rs_recv, back_send, back_recv,
+    chain, paired, cross, present, z_send, z_recv, ag_send, ag_recv, rs_send, rs_recv, back_send, back_recv,
 ):
     sp = lax.axis_index("sp")
     tp = lax.axis_index("tp")
     n_tp = 4
-    core = sp % 2
+    nz = n_sp // 2
+    z, core = sp // 2, sp % 2
     right, left = (tp + 1) % n_tp, (tp + n_tp - 1) % n_tp
     to_right, to_left = {"tp": right}, {"tp": left}
     last = n_sp - 1
     partner = sp + 1 - 2 * core
     across = sp - 1 + 2 * core
     has_across = (across >= 0) & (across <= last)
+    seat = (z - 1 + nz) % nz
+    is_late = seat >= nz - 2
+    mate = {"sp": core + 2 * (nz - 1) - 2 * jnp.where(z == 0, 0, nz - 1)}
     tok_dev = queries.shape[0]
     tok_sub, width = resid.shape
     cut = width // LANES
     unit = cap * cut
-    my_group, my_slot = sp // (n_sp // GROUPS), sp % (n_sp // GROUPS)
     own_pad = kk.shape[0] - 2 * WINDOW
-    slots = n_sp // GROUPS
-    half = slots // 2 * unit
-    whole = slots * unit
-    n_rows = n_tp * slots * cap
+    spans = [(2 * first, 2 * (end - first)) for first, end in groups_of(nz)]
+
+    def row_device(row):
+        return {"sp": 2 * row + core}
+
+    def seated(p, c):
+        return 2 * ((p + 1) % nz) + c
+
+    def region(g, part_of=None):
+        start, slots = spans[g]
+        if part_of is None:
+            return pl.ds(start * unit, slots * unit)
+        return pl.ds((start + part_of * (slots // 2)) * unit, slots // 2 * unit)
+
 
     loads = [
         pltpu.make_async_copy(out_proj_hbm, out_proj, load_sems.at[0]),
@@ -80,11 +102,25 @@
 
     tell(barrier, to_right)
     tell(barrier, to_left)
-    tell(barrier, {"sp": partner})
+    @pl.when(core == 1)
+    def _():
+        tell(barrier, {"sp": partner})
 
     @pl.when(has_across)
     def _():
         tell(barrier, {"sp": across})
+
+    @pl.when((seat > 0) & jnp.logical_not(is_late))
+    def _():
+        tell(barrier, row_device(z - 1))
+
+    @pl.when(is_late)
+    def _():
+        tell(barrier, row_device(nz - 2))
+
+    @pl.when(z == 0)
+    def _():
+        tell(barrier, mate)
 
     for load in loads:
         load.start()
@@ -115,7 +151,8 @@
     def _():
         blank(next_slot, 1)
 
-    pl.semaphore_wait(barrier, jnp.where(has_across, 4, 3))
+    expected = 3 + jnp.where(core == 0, 1, 0) + jnp.where(has_across, 1, 0)
+    pl.semaphore_wait(barrier, expected + jnp.where(seat == nz - 3, 1, 0) - jnp.where(z == 0, 1, 0))
 
     tail = pl.ds(tok_dev - WINDOW, WINDOW)
     head = pl.ds(0, WINDOW)
@@ -133,29 +170,49 @@
         ], 3)
     ]
 
+    @pl.when(core == 0)
+    def _():
+        tell(paired, {"sp": partner})
+
     @pl.when(sp < last)
     def _():
         for copy in halos_up:
             copy.start()
 
+    @pl.when(core == 1)
+    def _():
+        pl.semaphore_wait(paired, 1)
+
     @pl.when(sp > 0)
     def _():
         for copy in halos_down:
             copy.start()
 
-    @pl.when(sp > 0)
-    def _():
-        pl.semaphore_wait(chain, 1)
-
-    @pl.when(sp < last)
-    def _():
-        tell(chain, to_next)
-
-    def tell_below(d, carry):
-        tell(present.at[sp], {"sp": d})
+    def tell_earlier(p, carry):
+        for c in range(2):
+            tell(present.at[sp], {"sp": seated(p, c)})
         return carry
 
-    lax.fori_loop(0, sp, tell_below, 0)
+    @pl.when(z > 0)
+    def _():
+        @pl.when(seat > 0)
+        def _():
+            pl.semaphore_wait(chain, 1)
+
+        @pl.when(seat < nz - 3)
+        def _():
+            tell(chain, row_device(z + 1))
+
+        @pl.when(seat == nz - 3)
+        def _():
+            tell(chain, row_device(nz - 1))
+            tell(chain, row_device(0))
+
+        @pl.when(z == nz - 1)
+        def _():
+            tell(cross, mate)
+
+        lax.fori_loop(0, jnp.minimum(seat, nz - 2), tell_earlier, 0)
 
     ids = route_ids[...].astype(F32)
     sub_i = lax.broadcasted_iota(jnp.int32, (tok_sub, tok_sub), 0)
@@ -269,6 +326,14 @@
     proj_part[1, 1] = (proj_part[1, 1].astype(F32) + proj_in[1].astype(F32)).astype(BF16)
     c_left1 = remote(proj_part.at[1, 1], proj_right.at[1], proj_send.at[5], proj_recv.at[5], to_left)
     c_left1.start()
+
+    @pl.when(z == 0)
+    def _():
+        pl.semaphore_wait(chain, 1)
+        pl.semaphore_wait(cross, 1)
+        tell(cross, mate)
+        lax.fori_loop(0, nz - 2, tell_earlier, 0)
+
     project(tp, 0, 0)
     project(tp, 0, 1)
     for copy in (c_right1, c_left0, c_right0, c_left1):
@@ -289,27 +354,38 @@
         wide[pl.ds(c + 1, n_slots, stride=cut), :] = picked[:, LANES:]
     for e in range(n_sp):
         table[e] = wide[pl.ds(e * unit, unit), :].astype(BF16)
-    my_place = pl.ds(pl.multiple_of(my_slot * unit, unit), unit)
-    arrived[my_group, 0, my_place, :] = table[sp]
-
-    def dispatch(d):
-        remote(
-            table.at[d], arrived.at[my_group, 0, my_place], z_send.at[0], z_recv.at[sp], {"sp": d}
-        ).start()
-
-    def dispatch_down(i, carry):
-        dispatch(sp - i)
-        return carry
-
-    def dispatch_up(d, carry):
-        pl.semaphore_wait(present.at[d], 1)
-        dispatch(d)
-        return carry
-
-    lax.fori_loop(1, sp + 1, dispatch_down, 0)
-    lax.fori_loop(sp + 1, n_sp, dispatch_up, 0)
-
-    first, second = pl.ds(0, half), pl.ds(half, half)
+    arrived[0, pl.ds(0, unit), :] = table[sp]
+
+    def dispatch(g):
+        def one(i, carry):
+            o = jnp.where(i % 2 == 1, (i + 1) // 2, -(i // 2))
+            zd = (z + o + nz) % nz
+            place = pl.ds(pl.multiple_of((2 * i + core) * unit, unit), unit)
+            for c in range(2):
+                e = 2 * zd + c
+
+                @pl.when(jnp.logical_not(is_late) & ((zd + nz - 1) % nz > seat))
+                def _():
+                    pl.semaphore_wait(present.at[e], 1)
+
+                remote(
+                    table.at[e], arrived.at[0, place], z_send.at[0], z_recv.at[g], {"sp": e}
+                ).start()
+            return carry
+
+        start, slots = spans[g]
+        lax.fori_loop(max(start // 2, 1), (start + slots) // 2, one, 0)
+
+    @pl.when(z == nz - 1)
+    def _():
+        pl.semaphore_wait(cross, 1)
+
+    remote(
+        table.at[partner], arrived.at[0, pl.ds(unit, unit)], z_send.at[0], z_recv.at[0], {"sp": partner}
+    ).start()
+    dispatch(0)
+    dispatch(1)
+
     ag_copies, rs_copies = [], []
 
     def ag(i, g, src, dst, device):
@@ -325,37 +401,40 @@
     out_of = {}
 
     def step1(g):
-        for i in range(slots):
-            s = g * slots + i
-            place = arrived.at[g, 0, pl.ds(i * unit, unit)]
-
-            @pl.when(s != sp)
-            def _():
-                remote(place, place, z_send.at[0], z_recv.at[s], to_right).wait_recv()
-
-        a = ag(0, g, arrived.at[g, 0], arrived.at[g, 1], to_right)
+        start, slots = spans[g]
+        own = 1 if g == 0 else 0
+        landed = arrived.at[0, pl.ds((start + own) * unit, (slots - own) * unit)]
+        remote(landed, landed, z_send.at[0], z_recv.at[g], to_right).wait_recv()
+        whole = region(g)
+        a = ag(0, g, arrived.at[0, whole], arrived.at[1, whole], to_right)
         a.start()
-        b = ag(1, g, arrived.at[g, 0], arrived.at[g, 2], to_left)
+        b = ag(1, g, arrived.at[0, whole], arrived.at[2, whole], to_left)
         b.start()
         out_of["one", g] = (a, b)
 
     def step2(g):
         a, b = out_of["one", g]
+        first, second = region(g, 0), region(g, 1)
         a.wait_recv()
-        c = ag(2, g, arrived.at[g, 1, first], arrived.at[g, 3, first], to_right)
+        c = ag(2, g, arrived.at[1, first], arrived.at[3, first], to_right)
         c.start()
         b.wait_recv()
-        d = ag(3, g, arrived.at[g, 2, second], arrived.at[g, 3, second], to_left)
+        d = ag(3, g, arrived.at[2, second], arrived.at[3, second], to_left)
         d.start()
         out_of["two", g] = (c, d)
 
     def step3(g):
+        first, second, whole = region(g, 0), region(g, 1), region(g)
+        size = spans[g][1] * unit
+        n_rows = n_tp * spans[g][1] * cap
         for copy in out_of["two", g]:
             copy.wait_recv()
         for j in range(n_tp):
-            wide[pl.ds(j * whole, whole), :] = arrived[g, j].astype(F32)
+            wide[pl.ds(j * size, size), :] = arrived[j, whole, :].astype(F32)
         for c in range(cut):
-            rows[:, c * LANES : (c + 1) * LANES] = wide[pl.ds(c, n_rows, stride=cut), :].astype(BF16)
+            rows[0:n_rows, c * LANES : (c + 1) * LANES] = wide[
+                pl.ds(c, n_rows, stride=cut), :
+            ].astype(BF16)
         if g == 0:
             loads[1].wait()
             loads[2].wait()
@@ -364,63 +443,64 @@
 
         def act(n, carry):
             cols = pl.ds(pl.multiple_of(n * step, step), step)
-            a = jnp.dot(rows[...], gate[:, cols], preferred_element_type=F32)
-            b = jnp.dot(rows[...], up[:, cols], preferred_element_type=F32)
-            hidden[:, cols] = (a / (1.0 + jnp.exp(-a)) * b).astype(BF16)
+            a = jnp.dot(rows[0:n_rows, :], gate[:, cols], preferred_element_type=F32)
+            b = jnp.dot(rows[0:n_rows, :], up[:, cols], preferred_element_type=F32)
+            hidden[0:n_rows, cols] = (a / (1.0 + jnp.exp(-a)) * b).astype(BF16)
             return carry
 
         lax.fori_loop(0, hidden.shape[1] // step, act, 0)
         for n in range(cut // 2):
             y = jnp.dot(
-                hidden[...], down[:, n * 256 : (n + 1) * 256], preferred_element_type=F32
+                hidden[0:n_rows, :], down[:, n * 256 : (n + 1) * 256], preferred_element_type=F32
             )
             wide[pl.ds(2 * n, n_rows, stride=cut), :] = y[:, :LANES]
             wide[pl.ds(2 * n + 1, n_rows, stride=cut), :] = y[:, LANES:]
         for j in (3, 1, 2, 0):
-            part[g, j] = wide[pl.ds(j * whole, whole), :].astype(BF16)
-        a = rs(0, g, part.at[g, 3, first], sum_in.at[g, 0], to_right)
-        b = rs(1, g, part.at[g, 3, second], sum_in.at[g, 1], to_left)
-        c = rs(2, g, part.at[g, 2, second], from_left.at[g, second], to_right)
-        d = rs(3, g, part.at[g, 1, first], from_right.at[g, first], to_left)
+            part[j, whole, :] = wide[pl.ds(j * size, size), :].astype(BF16)
+        a = rs(0, g, part.at[3, first], sum_in.at[first], to_right)
+        b = rs(1, g, part.at[3, second], sum_in.at[second], to_left)
+        c = rs(2, g, part.at[2, second], from_left.at[second], to_right)
+        d = rs(3, g, part.at[1, first], from_right.at[first], to_left)
         for copy in (a, b, c, d):
             copy.start()
         out_of["three", g] = (a, b, c, d)
 
     def step4(g):
         a, b, c, d = out_of["three", g]
+        first, second = region(g, 0), region(g, 1)
         a.wait_recv()
-        part[g, 2, first, :] = (part[g, 2, first, :].astype(F32) + sum_in[g, 0].astype(F32)).astype(BF16)
-        e = rs(4, g, part.at[g, 2, first], from_left.at[g, first], to_right)
+        part[2, first, :] = (part[2, first, :].astype(F32) + sum_in[first, :].astype(F32)).astype(BF16)
+        e = rs(4, g, part.at[2, first], from_left.at[first], to_right)
         e.start()
         b.wait_recv()
-        part[g, 1, second, :] = (part[g, 1, second, :].astype(F32) + sum_in[g, 1].astype(F32)).astype(BF16)
-        f = rs(5, g, part.at[g, 1, second], from_right.at[g, second], to_left)
+        part[1, second, :] = (part[1, second, :].astype(F32) + sum_in[second, :].astype(F32)).astype(BF16)
+        f = rs(5, g, part.at[1, second], from_right.at[second], to_left)
         f.start()
         out_of["four", g] = (c, d, e, f)
 
     def step5(g):
+        whole = region(g)
         for copy in out_of["four", g]:
             copy.wait_recv()
-        result[g] = (
-            part[g, 0].astype(F32) + from_left[g].astype(F32) + from_right[g].astype(F32)
+        result[whole, :] = (
+            part[0, whole, :].astype(F32) + from_left[whole, :].astype(F32) + from_right[whole, :].astype(F32)
         ).astype(BF16)
-        for i in range(slots):
-            s = g * slots + i
-            src = pl.ds(i * unit, unit)
-
-            @pl.when(s != sp)
-            def _():
+        start, slots = spans[g]
+        for q in range(start, start + slots):
+            src = pl.ds(q * unit, unit)
+            if q == 0:
+                returned[sp] = result[src, :]
+            else:
+                peer = partner if q == 1 else 2 * ((z - offset_of(q // 2) + nz) % nz) + q % 2
                 remote(
-                    result.at[g, src], returned.at[sp], back_send.at[0], back_recv.at[0], {"sp": s}
+                    result.at[src], returned.at[sp], back_send.at[0], back_recv.at[0], {"sp": peer}
                 ).start()
 
-            @pl.when(s == sp)
-            def _():
-                returned[sp] = result[g, src, :]
-
     step1(0)
+    dispatch(2)
     step2(0)
     step1(1)
+    dispatch(3)
     step3(0)
     step2(1)
     step1(2)
@@ -431,8 +511,8 @@
     step4(1)
     step1(3)
     step3(2)
+    step2(3)
     step5(1)
-    step2(3)
     step4(2)
     step3(3)
     step5(2)
@@ -484,10 +564,9 @@
     cut = width // LANES
     unit = cap * cut
     own_pad = -(-tok_dev // LANES) * LANES
-    slots = n_sp // GROUPS
-    whole = slots * unit
-    half = whole // 2
-    n_rows = 4 * slots * cap
+    groups = len(groups_of(n_sp // 2))
+    most = 2 * max(end - first for first, end in groups_of(n_sp // 2))
+    n_rows = -(-4 * most * cap // 16) * 16
     vmem = pl.BlockSpec(memory_space=pltpu.VMEM)
     hbm = pl.BlockSpec(memory_space=pl.ANY)
     dma = pltpu.SemaphoreType.DMA
@@ -506,22 +585,23 @@
         pltpu.VMEM((2, tok_sub, width // 2), BF16),
         pltpu.VMEM((2, tok_sub, width // 2), BF16),
         pltpu.VMEM((tok_sub, width), BF16),
-        pltpu.VMEM((max(n_sp * unit, 4 * whole), LANES), F32),
+        pltpu.VMEM((max(n_sp, 4 * most) * unit, LANES), F32),
         pltpu.VMEM((n_sp, unit, LANES), BF16),
-        pltpu.VMEM((GROUPS, 4, whole, LANES), BF16),
+        pltpu.VMEM((4, n_sp * unit, LANES), BF16),
         pltpu.VMEM((n_rows, width), BF16),
         pltpu.VMEM((n_rows, ff), BF16),
-        pltpu.VMEM((GROUPS, 4, whole, LANES), BF16),
-        pltpu.VMEM((GROUPS, 2, half, LANES), BF16),
-        pltpu.VMEM((GROUPS, whole, LANES), BF16),
-        pltpu.VMEM((GROUPS, whole, LANES), BF16),
-        pltpu.VMEM((GROUPS, whole, LANES), BF16),
+        pltpu.VMEM((4, n_sp * unit, LANES), BF16),
+        pltpu.VMEM((n_sp * unit, LANES), BF16),
+        pltpu.VMEM((n_sp * unit, LANES), BF16),
+        pltpu.VMEM((n_sp * unit, LANES), BF16),
+        pltpu.VMEM((n_sp * unit, LANES), BF16),
         pltpu.VMEM((n_sp, unit, LANES), BF16),
         pltpu.VMEM((tok_sub, width), F32),
         dma((4,)), dma((6,)), dma((6,)), dma((6,)), dma((6,)),
+        pltpu.SemaphoreType.REGULAR, pltpu.SemaphoreType.REGULAR,
         pltpu.SemaphoreType.REGULAR, pltpu.SemaphoreType.REGULAR((n_sp,)),
-        dma((1,)), dma((n_sp,)), dma((4, GROUPS)), dma((4, GROUPS)),
-        dma((6, GROUPS)), dma((6, GROUPS)), dma((1,)), dma((1,)),
+        dma((1,)), dma((groups,)), dma((4, groups)), dma((4, groups)),
+        dma((6, groups)), dma((6, groups)), dma((1,)), dma((1,)),
     ]
     flops = 2 * tok_dev * att * width + 2 * 4 * tok_sub * 2 * width * ff * 3
     return pl.pallas_call(

time: 104 us -> 99.4 us (0.956)
  the two profiles are of different devices: /device:TPU:33 before, /device:TPU:40 now
where the time goes in v3:
time: 99.4 us; the launch traced here: 98.8 us
  Pallas kernels  97.1 us (98%)
  local copies, waits for them, and re-layouts  1.62 us (2%)
    pallas_call x1, Pallas kernels, per_device(): pl.pallas_call(functools.partial(kernel, n_sp, cap), out_shape=jax.ShapeD...  97.1 us

profile of v3, /device:TPU:40, one launch (start us, length us, event | category | flops | bytes accessed | tf_op | source)
XLA Modules:
  0.0 98.8 jit_solution(15875108034119530723)
XLA Ops:
  0.0 97.1 %layer.1 = bf16[48,2048]{1,0:T(8,128)(2,1)} custom-call(bf16[48,2048]{1,0:T(8,128)(2,1)} %resid.1, bf16[192,256]{1,0:T(8,128)(2,1)} %queries.1, bf16[64,192]{1,0:T(8,128)(2,1)} %bitcast.9, bf16[64,192]{1,0:T(8,128)(2,1)} %bitcast.10, s32[1,192]{1,0:T(1,128)} %bitcast.15, f32[4]{0:T(128)} %sinks.1, bf16[256,2048]{1,0:T(8,128)(2,1)} %out_proj_hbm.1, ...), custom_call_target="tpu_custom_call" | custom-call | flops 3825205248 | bytes 12000000 | tf_op jit(solution)/shard_map/layer/pallas_call | solution.py:607
  97.2 1.6 %copy.18 = bf16[48,2048]{1,0:T(8,128)(2,1)} copy(bf16[48,2048]{1,0:T(8,128)(2,1)} %layer.1) | data formatting | bytes 393216

commit v4 on v3

--- a/solution.py
+++ b/solution.py
@@ -369,7 +369,7 @@
                     pl.semaphore_wait(present.at[e], 1)
 
                 remote(
-                    table.at[e], arrived.at[0, place], z_send.at[0], z_recv.at[g], {"sp": e}
+                    table.at[e], arrived.at[0, place], z_send.at[g], z_recv.at[g], {"sp": e}
                 ).start()
             return carry
 
@@ -383,7 +383,13 @@
     remote(
         table.at[partner], arrived.at[0, pl.ds(unit, unit)], z_send.at[0], z_recv.at[0], {"sp": partner}
     ).start()
+    def sent(g):
+        count = spans[g][1] - (1 if g == 0 else 0)
+        cells = table.at[pl.ds(0, count)]
+        remote(cells, cells, z_send.at[g], z_recv.at[g], to_right).wait_send()
+
     dispatch(0)
+    sent(0)
     dispatch(1)
 
     ag_copies, rs_copies = [], []
@@ -548,7 +554,8 @@
         copy.wait_send()
     for copy in ag_copies + rs_copies:
         copy.wait_send()
-    remote(others, others, z_send.at[0], z_recv.at[0], to_right).wait_send()
+    for g in range(1, len(spans)):
+        sent(g)
     remote(others, others, back_send.at[0], back_recv.at[0], to_right).wait_send()
 
 
@@ -600,7 +607,7 @@
         dma((4,)), dma((6,)), dma((6,)), dma((6,)), dma((6,)),
         pltpu.SemaphoreType.REGULAR, pltpu.SemaphoreType.REGULAR,
         pltpu.SemaphoreType.REGULAR, pltpu.SemaphoreType.REGULAR((n_sp,)),
-        dma((1,)), dma((groups,)), dma((4, groups)), dma((4, groups)),
+        dma((groups,)), dma((groups,)), dma((4, groups)), dma((4, groups)),
         dma((6, groups)), dma((6, groups)), dma((1,)), dma((1,)),
     ]
     flops = 2 * tok_dev * att * width + 2 * 4 * tok_sub * 2 * width * ff * 3

time: 99.4 us -> 99 us (level)
  no operation moved by 1% of the time
where the time goes in v4:
time: 99 us; the launch traced here: 98.7 us
  Pallas kernels  97.1 us (98%)
  local copies, waits for them, and re-layouts  1.62 us (2%)
    pallas_call x1, Pallas kernels, per_device(): pl.pallas_call(functools.partial(kernel, n_sp, cap), out_shape=jax.ShapeD...  97.1 us

profile of v4, /device:TPU:40, one launch (start us, length us, event | category | flops | bytes accessed | tf_op | source)
XLA Modules:
  0.0 98.7 jit_solution(5310544991765453298)
XLA Ops:
  0.0 97.1 %layer.1 = bf16[48,2048]{1,0:T(8,128)(2,1)} custom-call(bf16[48,2048]{1,0:T(8,128)(2,1)} %resid.1, bf16[192,256]{1,0:T(8,128)(2,1)} %queries.1, bf16[64,192]{1,0:T(8,128)(2,1)} %bitcast.9, bf16[64,192]{1,0:T(8,128)(2,1)} %bitcast.10, s32[1,192]{1,0:T(1,128)} %bitcast.15, f32[4]{0:T(128)} %sinks.1, bf16[256,2048]{1,0:T(8,128)(2,1)} %out_proj_hbm.1, ...), custom_call_target="tpu_custom_call" | custom-call | flops 3825205248 | bytes 12000000 | tf_op jit(solution)/shard_map/layer/pallas_call | solution.py:614
  97.1 1.6 %copy.18 = bf16[48,2048]{1,0:T(8,128)(2,1)} copy(bf16[48,2048]{1,0:T(8,128)(2,1)} %layer.1) | data formatting | bytes 393216

commit v5 on v4

--- a/solution.py
+++ b/solution.py
@@ -20,8 +20,8 @@
 
 def groups_of(nz):
     base, extra = nz // 4, nz // 16
-    edges = (0, base + extra, 2 * base + extra, 3 * base + extra, nz)
-    return tuple(zip(edges[:-1], edges[1:]))
+    one, two, three = base + extra, 2 * base + extra, 3 * base + extra
+    return ((0, one), (one, two), (three, nz), (two, three))
 
 
 def offset_of(i):

time: 99 us -> 99.2 us (level)
  no operation moved by 1% of the time
where the time goes in v5:
time: 99.2 us; the launch traced here: 98.7 us
  Pallas kernels  97.1 us (98%)
  local copies, waits for them, and re-layouts  1.62 us (2%)
    pallas_call x1, Pallas kernels, per_device(): pl.pallas_call(functools.partial(kernel, n_sp, cap), out_shape=jax.ShapeD...  97.1 us

profile of v5, /device:TPU:40, one launch (start us, length us, event | category | flops | bytes accessed | tf_op | source)
XLA Modules:
  0.0 98.7 jit_solution(12181818810129334588)
XLA Ops:
  0.0 97.1 %layer.1 = bf16[48,2048]{1,0:T(8,128)(2,1)} custom-call(bf16[48,2048]{1,0:T(8,128)(2,1)} %resid.1, bf16[192,256]{1,0:T(8,128)(2,1)} %queries.1, bf16[64,192]{1,0:T(8,128)(2,1)} %bitcast.9, bf16[64,192]{1,0:T(8,128)(2,1)} %bitcast.10, s32[1,192]{1,0:T(1,128)} %bitcast.15, f32[4]{0:T(128)} %sinks.1, bf16[256,2048]{1,0:T(8,128)(2,1)} %out_proj_hbm.1, ...), custom_call_target="tpu_custom_call" | custom-call | flops 3825205248 | bytes 12000000 | tf_op jit(solution)/shard_map/layer/pallas_call | solution.py:614
  97.1 1.6 %copy.18 = bf16[48,2048]{1,0:T(8,128)(2,1)} copy(bf16[48,2048]{1,0:T(8,128)(2,1)} %layer.1) | data formatting | bytes 393216
